TPU v7x, 32 devices: a whole 2x2x4 slice. The times are simulated.
32 devices in a mesh: grp: 2 (over y), fs: 4 (over z), tp: 4 (over x, core).
Axes of the slice: x: 2, y: 2, z: 4, core: 2. Of those that a mesh axis runs over, the one named last changes fastest.
Arguments:
- tokens: bfloat16 [4096, 2048], P(('grp', 'fs')), parts along dimension 0, may hold values from -6 to 6
- norm_in: bfloat16 [2048], replicated, may hold values from 0.099609375 to 1.8984375
- w_value: bfloat16 [2048, 2048], P('fs', 'tp'), may hold values from -0.125 to 0.125
- w_gate: bfloat16 [2048, 2048], P('fs', 'tp'), may hold values from -0.125 to 0.125
- conv_kernel: float32 [31, 2048], replicated, as said below
- ln_gain: bfloat16 [2048], replicated, may hold values from 0.099609375 to 1.8984375
- ln_shift: bfloat16 [2048], replicated, may hold values from -3 to 3
- w_out: bfloat16 [2048, 2048], P('tp', 'fs'), may hold values from -0.125 to 0.125
- norm_mlp: bfloat16 [2048], replicated, may hold values from 0.099609375 to 1.8984375
- w_up: bfloat16 [2048, 8192], P('fs', 'tp'), may hold values from -0.125 to 0.125
- w_down: bfloat16 [8192, 2048], P('tp', 'fs'), may hold values from -0.0625 to 0.0625
Outputs:
- layer_out: bfloat16 [4096, 2048], P(('grp', 'fs', 'tp')), parts along dimension 0
There are 2 independent parts, one for each index of `grp`. A program takes and returns all parts, laid end to end along the dimension named above; an argument that names none is the same for every part. Nothing has to cross between parts.
Inputs may be any that keep to these rules, and one draw needn't show every extreme that they name: `conv_kernel`: a depthwise kernel.
All inputs are finite; a program needn't handle non-finite values.
Results may differ from a plain program's by a relative error of at most 0.018.
Values may be sent and summed in bfloat16 or wider, within the bound.
A program may use at most 64 MiB of HBM per device.

v0:
```python
import functools

import jax
import jax.numpy as jnp
from jax import lax
from jax.experimental import pallas as pl
from jax.experimental.pallas import tpu as pltpu
from jax.sharding import PartitionSpec as P

MESH = pl.DeviceIdType.MESH
PIECES = 4
AHEAD = 3
PAD = 32


def rms_rows(x, gain):
    return x * lax.rsqrt(jnp.mean(x * x, axis=-1, keepdims=True) + 1e-06) * gain


def kernel(
    F, T,
    tok, norm_in, conv_k, ln_gain, ln_shift, norm_mlp, wv, wg, wo, wu, wd,
    out,
    normed, gv, gg, go, gu, gd, gated, conv, act, part, rs, resid, nm, hidden, fin, rs2,
    nm_e, hid_e, fin_e, rs_e, sum_e, ret,
    st_own, st_recv, nm_own,
    local_sem, zsend_r, zsend_l, zrecv_r, zrecv_l, ysend_r, ysend_l, yrecv_r, yrecv_l,
    st_send, st_rsem, rs_send, rs_rsem, ag_send, ag_rsem, fs_send, fs_rsem,
    rest, ex_sem, ea_send, ea_rsem, fe_send, fe_rsem, ret_send, ret_rsem,
):
    g = lax.axis_index("grp")
    z = lax.axis_index("fs")
    t = lax.axis_index("tp")
    S, D = tok.shape
    R, C = wv.shape
    H = wu.shape[1]
    N = wo.shape[1]
    taps = conv_k.shape[0]
    rows = S // T
    R2, C2, H2 = R // 2, C // 2, H // 2
    HB, HC = H // PIECES, H2 // PIECES
    other = 1 - g
    n_chunks = 3 + 2 * PIECES
    first_down = 3 + PIECES

    LOW = PIECES // 2
    HL = LOW * HB
    at_left, at_right = z == 0, z == F - 1
    is_end = jnp.logical_or(at_left, at_right)
    help_left, help_right = z == 1, z == F - 2

    def upper(c):
        return c >= 3 and (c - 3) % PIECES >= LOW

    def when_right(c):
        return pl.when(z < F - 1 - upper(c))

    def when_left(c):
        return pl.when(z > 0 + upper(c))

    def for_ends(body):
        @pl.when(at_left)
        def _():
            body(z + 1)

        @pl.when(at_right)
        def _():
            body(z - 1)

    def for_helpers(body):
        @pl.when(help_left)
        def _():
            body(z - 1)

        @pl.when(help_right)
        def _():
            body(z + 1)

    def mult(i, k):
        return pl.multiple_of(i, k)

    def own(c, h):
        if c < 3:
            ref, size = ((wv, R2), (wg, R2), (wo, C2))[c]
            return ref.at[pl.ds(mult(h * size, size), size), :]
        if c < first_down:
            return wu.at[pl.ds(mult(h * R2, R2), R2), pl.ds((c - 3) * HB, HB)]
        return wd.at[pl.ds(mult((c - first_down) * HB + h * HC, HC), HC), :]

    def slot(c, src, h):
        if c < 2:
            return (gv, gg)[c].at[pl.ds(mult(src * R + h * R2, R2), R2), :]
        if c == 2:
            return go.at[src, pl.ds(mult(h * C2, C2), C2), :]
        if c < first_down:
            return gu.at[c - 3, pl.ds(mult(src * R + h * R2, R2), R2), :]
        return gd.at[src, pl.ds(mult((c - first_down) * HB + h * HC, HC), HC), :]

    def remote(src_ref, dst_ref, send, recv, device):
        return pltpu.make_async_remote_copy(
            src_ref=src_ref, dst_ref=dst_ref, send_sem=send, recv_sem=recv,
            device_id=device, device_id_type=MESH,
        )

    peers = [lax.rem(t + i, T) for i in range(T)]
    sources = [lax.rem(t - i + T, T) for i in range(T)]

    barrier = pltpu.get_barrier_semaphore()

    def greet(device):
        pl.semaphore_signal(barrier, inc=1, device_id=device, device_id_type=MESH)

    greet((other, z, t))
    for i in range(1, T):
        greet((g, z, peers[i]))

    @pl.when(z > 0)
    def _():
        greet((g, z - 1, t))

    @pl.when(z < F - 1)
    def _():
        greet((g, z + 1, t))

    ends = lax.div(z + F - 1, F) + lax.div(2 * F - 2 - z, F)
    pl.semaphore_wait(barrier, T + ends)

    ys, yr = (ysend_r, ysend_l), (yrecv_r, yrecv_l)

    def own_right(c):
        return remote(own(c, g), slot(c, z, g), zsend_r.at[c, 0], zrecv_r.at[c, 1], (g, z + 1, t))

    def own_left(c):
        return remote(own(c, g), slot(c, z, g), zsend_l.at[c, 0], zrecv_l.at[c, 1], (g, z - 1, t))

    def right_hop(c, d, src):
        return remote(slot(c, src, g), slot(c, src, g), zsend_r.at[c, d], zrecv_r.at[c, min(d + 1, F - 1)], (g, z + 1, t))

    def left_hop(c, d, src):
        return remote(slot(c, src, g), slot(c, src, g), zsend_l.at[c, d], zrecv_l.at[c, min(d + 1, F - 1)], (g, z - 1, t))

    def arrival(c, d, src, left):
        sems = zrecv_l if left else zrecv_r
        return remote(slot(c, src, g), slot(c, src, g), zsend_r.at[c, d], sems.at[c, d], (g, z, t))

    def across(c, d, src, left):
        return remote(slot(c, src, g), slot(c, src, g), ys[left].at[c, d], yr[left].at[c, d], (other, z, t))

    def across_arrival(c, d, src, left):
        return remote(slot(c, src, other), slot(c, src, other), ys[left].at[c, d], yr[left].at[c, d], (other, z, t))

    def own_rest(c, helper):
        return remote(own(c, other), slot(c, z, other), ex_sem.at[2 + c], rest.at[c], (g, helper, t))

    issued = [0]

    def own_upto(limit):
        while issued[0] < min(limit, n_chunks):
            c = issued[0]
            issued[0] += 1

            @when_right(c)
            def _():
                own_right(c).start()

            @when_left(c)
            def _():
                own_left(c).start()

            for_ends(lambda helper: own_rest(c, helper).start())

    def both(d, body, c=0):
        @pl.when(jnp.logical_and(z - d >= 0, z < F - upper(c)))
        def _():
            body(z - d, 0)

        @pl.when(jnp.logical_and(z + d < F, z >= 0 + upper(c)))
        def _():
            body(z + d, 1)

    def when_across(d, left):
        if d > 1:
            return lambda body: body()
        return pl.when(z != (F - 2 if left else 1))

    def forward(c, d, src, left, act_on):
        if d < F - 1:
            if left:
                @when_left(c)
                def _():
                    act_on(left_hop(c, d, src))
            else:
                @when_right(c)
                def _():
                    act_on(right_hop(c, d, src))

        @when_across(d, left)
        def _():
            act_on(across(c, d, src, left))

    def service(c, d):
        def body(src, left):
            arrival(c, d, src, left).wait_recv()
            forward(c, d, src, left, lambda copy: copy.start())

        both(d, body, c)

    def service_all(c):
        own_upto(c + 1 + AHEAD)
        for d in range(1, F):
            service(c, d)

    def y_wait(c, d):
        def body(src, left):
            @when_across(d, left)
            def _():
                across_arrival(c, d, src, left).wait_recv()

            if d == 1:
                @pl.when(z == (F - 2 if left else 1))
                def _():
                    remote(slot(c, src, other), slot(c, src, other), ex_sem.at[0], rest.at[c], (g, src, t)).wait_recv()

        both(d, body, c)

    def y_wait_all(c):
        for d in range(1, F):
            y_wait(c, d)

    own_upto(1)
    copies = [
        pltpu.make_async_copy(wv, gv.at[pl.ds(mult(z * R, R), R), :], local_sem.at[0]),
        pltpu.make_async_copy(wg, gg.at[pl.ds(mult(z * R, R), R), :], local_sem.at[1]),
        pltpu.make_async_copy(wo, go.at[z], local_sem.at[2]),
        pltpu.make_async_copy(wd, gd.at[z], local_sem.at[3]),
    ]
    for j in range(PIECES):
        copies.append(
            pltpu.make_async_copy(
                wu.at[:, pl.ds(j * HB, HB)], gu.at[j, pl.ds(mult(z * R, R), R), :], local_sem.at[4 + j]
            )
        )
    for copy in copies:
        copy.start()
    own_upto(1 + AHEAD)

    block = 64

    def norm_step(i, carry):
        at = pl.ds(mult(i * block, block), block)
        x = tok[at, :].astype(jnp.float32)
        normed[at, :] = rms_rows(x, norm_in[...].astype(jnp.float32)).astype(jnp.bfloat16)
        return carry

    lax.fori_loop(0, S // block, norm_step, 0)
    for copy in copies:
        copy.wait()

    service_all(0)
    service_all(1)
    own_upto(3 + AHEAD)
    service(2, 1)
    y_wait_all(0)
    y_wait_all(1)

    tile = min(256, C)
    gated[0:PAD, :] = jnp.zeros((PAD, C), jnp.float32)

    def gate_step(i, carry):
        at = pl.ds(mult(i * tile, tile), tile)
        v = jnp.dot(normed[...], gv[:, at], preferred_element_type=jnp.float32)
        a = jnp.dot(normed[...], gg[:, at], preferred_element_type=jnp.float32)
        gated[PAD:, at] = v * jax.nn.sigmoid(a)
        return carry

    lax.fori_loop(0, C // tile, gate_step, 0)

    for d in range(2, F):
        service(2, d)

    span = 128
    lead = PAD - (taps - 1)

    def conv_step(i, carry):
        base = mult(i * span, span)
        first = jnp.zeros((span, 128), jnp.float32)
        second = jnp.zeros((span, 128), jnp.float32)
        for j in range(C // 128):
            lanes = pl.ds(j * 128, 128)
            window = gated[pl.ds(base, span + PAD), lanes]
            weights = conv_k[:, pl.ds(mult(t * C + j * 128, 128), 128)]
            acc = jnp.zeros((span, 128), jnp.float32)
            for k in range(taps):
                acc = acc + weights[k : k + 1, :] * window[lead + k : lead + k + span, :]
            conv[pl.ds(base, span), lanes] = acc
            first = first + acc
            second = second + acc * acc
        lane = lax.broadcasted_iota(jnp.int32, (span, 128), 1)
        both_sums = jnp.where(
            lane == 0,
            jnp.sum(first, axis=1, keepdims=True),
            jnp.where(lane == 1, jnp.sum(second, axis=1, keepdims=True), 0.0),
        )
        st_own[:, pl.ds(base, span)] = jnp.transpose(both_sums)[0:8, :]
        return carry

    lax.fori_loop(0, S // span, conv_step, 0)

    def stat_copy(i):
        return remote(st_own, st_recv.at[i], st_send.at[i], st_rsem.at[i], (g, z, peers[i]))

    for i in range(1, T):
        stat_copy(i).start()
    service_all(3)
    for i in range(1, T):
        stat_copy(i).wait_recv()

    gain = ln_gain[:, pl.ds(mult(t * C, C), C)].astype(jnp.float32)
    shift = ln_shift[:, pl.ds(mult(t * C, C), C)].astype(jnp.float32)

    def act_step(i, carry):
        base = mult(i * span, span)
        at = pl.ds(base, span)
        sums = st_own[:, at]
        for k in range(1, T):
            sums = sums + st_recv[k, :, at]
        mean = sums[0:1, :] / D
        var = sums[1:2, :] / D - mean * mean
        scale = lax.rsqrt(var + 1e-05)
        mean_c = jnp.transpose(jnp.broadcast_to(mean, (128, span)))[:, 0:1]
        scale_c = jnp.transpose(jnp.broadcast_to(scale, (128, span)))[:, 0:1]
        n = (conv[at, :] - mean_c) * scale_c * gain + shift
        act[at, :] = (n * jax.nn.sigmoid(n)).astype(jnp.bfloat16)
        return carry

    lax.fori_loop(0, S // span, act_step, 0)
    y_wait_all(2)

    def out_step(i, carry):
        part[:, pl.ds(mult(i * N, N), N)] = jnp.dot(
            act[...], go[i], preferred_element_type=jnp.float32
        ).astype(jnp.bfloat16)
        return carry

    lax.fori_loop(0, F, out_step, 0)

    def mix_copy(i):
        return remote(
            part.at[pl.ds(mult(peers[i] * rows, rows), rows), :], rs.at[i], rs_send.at[i], rs_rsem.at[i], (g, z, peers[i])
        )

    for i in range(1, T):
        mix_copy(i).start()
    service_all(4)
    service(5, 1)
    for i in range(1, T):
        mix_copy(i).wait_recv()

    small = 32

    def resid_step(i, carry):
        at = pl.ds(mult(i * small, small), small)
        mine = pl.ds(mult(t * rows + i * small, small), small)
        total = part[mine, :].astype(jnp.float32)
        for k in range(1, T):
            total = total + rs[k, at, :].astype(jnp.float32)
        r = tok[mine, :].astype(jnp.float32) + total
        resid[at, :] = r
        nm_own[at, :] = rms_rows(r, norm_mlp[...].astype(jnp.float32)).astype(jnp.bfloat16)
        return carry

    lax.fori_loop(0, rows // small, resid_step, 0)

    def norm_copy(i):
        return remote(
            nm_own, nm.at[pl.ds(mult(t * rows, rows), rows), :], ag_send.at[i], ag_rsem.at[i], (g, z, peers[i])
        )

    def norm_arrival(i):
        return remote(
            nm_own, nm.at[pl.ds(mult(sources[i] * rows, rows), rows), :], ag_send.at[i], ag_rsem.at[i], (g, z, peers[i])
        )

    for i in range(1, T):
        norm_copy(i).start()
    mine = pl.ds(mult(t * rows, rows), rows)

    def give_copy(helper):
        return remote(nm_own, nm_e.at[mine, :], ex_sem.at[0], ex_sem.at[1], (g, helper, t))

    for_ends(lambda helper: give_copy(helper).start())
    nm[mine, :] = nm_own[...]
    own_upto(5 + 1 + AHEAD)
    for d in range(2, F):
        service(5, d)
    service_all(6)
    own_upto(n_chunks)

    def share_copy(i):
        return remote(nm_e.at[mine, :], nm_e.at[mine, :], ea_send.at[i], ea_rsem.at[i], (g, z, peers[i]))

    def share_arrival(i):
        there = pl.ds(mult(sources[i] * rows, rows), rows)
        return remote(nm_e.at[there, :], nm_e.at[there, :], ea_send.at[i], ea_rsem.at[i], (g, z, peers[i]))

    def share(end):
        remote(nm_own, nm_e.at[mine, :], ex_sem.at[0], ex_sem.at[1], (g, end, t)).wait_recv()
        for i in range(1, T):
            share_copy(i).start()

    for_helpers(share)
    for i in range(1, T):
        norm_arrival(i).wait_recv()

    utile = min(256, HB)

    def up_block(j):
        y_wait_all(3 + j)

        def up_step(i, carry):
            at = pl.ds(mult(i * utile, utile), utile)
            a = jnp.dot(nm[...], gu[j, :, at], preferred_element_type=jnp.float32)
            a = jnp.maximum(a, 0.0)
            hidden[:, pl.ds(mult(j * HB + i * utile, utile), utile)] = (a * a).astype(jnp.bfloat16)
            return carry

        lax.fori_loop(0, HB // utile, up_step, 0)

    def up_some(j):
        if j < LOW:
            up_block(j)
        else:
            @pl.when(jnp.logical_not(is_end))
            def _():
                up_block(j)

    for j in range(PIECES):
        if j < PIECES - 1:
            up_some(j)
        service(first_down + j, 1)
    up_some(PIECES - 1)

    def up_for_end(end):
        for i in range(1, T):
            share_arrival(i).wait_recv()
        per = HB // utile

        def up_step(i, carry):
            at = pl.ds(mult(lax.rem(i, per) * utile, utile), utile)
            a = jnp.dot(nm_e[...], gu[LOW + lax.div(i, per), :, at], preferred_element_type=jnp.float32)
            a = jnp.maximum(a, 0.0)
            hid_e[:, pl.ds(mult(i * utile, utile), utile)] = (a * a).astype(jnp.bfloat16)
            return carry

        lax.fori_loop(0, (PIECES - LOW) * per, up_step, 0)

    for_helpers(up_for_end)

    ntile = min(256, N)

    def fin_copy(src, i):
        return remote(
            fin.at[src, pl.ds(mult(peers[i] * rows, rows), rows), :], rs2.at[src, i],
            fs_send.at[src, i], fs_rsem.at[src, i], (g, z, peers[i]),
        )

    def end_copy(src, i):
        return remote(
            fin_e.at[src, pl.ds(mult(peers[i] * rows, rows), rows), :], rs_e.at[src, i],
            fe_send.at[src, i], fe_rsem.at[src, i], (g, z, peers[i]),
        )

    def down_for_end(src):
        def down_step(i, carry):
            at = pl.ds(mult(i * ntile, ntile), ntile)
            fin_e[src, :, at] = jnp.dot(
                hid_e[...], gd[src, HL:, at], preferred_element_type=jnp.float32
            ).astype(jnp.bfloat16)
            return carry

        lax.fori_loop(0, N // ntile, down_step, 0)
        for i in range(1, T):
            end_copy(src, i).start()

    def ret_copy(src, end):
        return remote(sum_e.at[src], ret.at[src], ret_send.at[src], ret_rsem.at[src], (g, end, t))

    def return_sum(src):
        def body(end):
            for i in range(1, T):
                end_copy(src, i).wait_recv()
            total = fin_e[src, mine, :].astype(jnp.float32)
            for k in range(1, T):
                total = total + rs_e[src, k].astype(jnp.float32)
            sum_e[src] = total.astype(jnp.bfloat16)
            ret_copy(src, end).start()

        for_helpers(body)

    def down(src):
        for_helpers(lambda end: down_for_end(src))

        def rows_to(limit):
            def down_step(i, carry):
                at = pl.ds(mult(i * ntile, ntile), ntile)
                fin[src, :, at] = jnp.dot(
                    hidden[:, :limit], gd[src, :limit, at], preferred_element_type=jnp.float32
                ).astype(jnp.bfloat16)
                return carry

            lax.fori_loop(0, N // ntile, down_step, 0)

        @pl.when(is_end)
        def _():
            rows_to(HL)

        @pl.when(jnp.logical_not(is_end))
        def _():
            rows_to(H)

        for i in range(1, T):
            fin_copy(src, i).start()

    def finish(src):
        for i in range(1, T):
            fin_copy(src, i).wait_recv()
        cols = pl.ds(mult(src * N, N), N)
        total = fin[src, mine, :].astype(jnp.float32)
        for k in range(1, T):
            total = total + rs2[src, k].astype(jnp.float32)
        resid[:, cols] = resid[:, cols] + total

    down(z)
    for d in range(1, F):
        if d + 1 < F:
            service(first_down, d + 1)
        for c in range(first_down, n_chunks):
            y_wait(c, d)
        both(d, lambda src, left: down(src))
        if d + 1 < F:
            for c in range(first_down + 1, n_chunks):
                service(c, d + 1)
        if d == 1:
            return_sum(z)
        else:
            both(d - 1, lambda src, left: return_sum(src))
    both(F - 1, lambda src, left: return_sum(src))

    def finish_step(src, carry):
        finish(src)

        def add(helper):
            cols = pl.ds(mult(src * N, N), N)
            ret_copy(src, helper).wait_recv()
            resid[:, cols] = resid[:, cols] + ret[src].astype(jnp.float32)

        for_ends(add)
        cols = pl.ds(mult(src * N, N), N)
        out[:, cols] = resid[:, cols].astype(jnp.bfloat16)
        return carry

    lax.fori_loop(0, F, finish_step, 0)

    for c in range(n_chunks):
        @when_right(c)
        def _():
            own_right(c).wait_send()

        @when_left(c)
        def _():
            own_left(c).wait_send()

        for_ends(lambda helper: own_rest(c, helper).wait_send())

        for d in range(1, F):
            both(d, lambda src, left: forward(c, d, src, left, lambda copy: copy.wait_send()), c)

    for_ends(lambda helper: give_copy(helper).wait_send())

    def drain_helper(end):
        for i in range(1, T):
            share_copy(i).wait_send()
            for src in range(F):
                end_copy(src, i).wait_send()
        for src in range(F):
            ret_copy(src, end).wait_send()

    for_helpers(drain_helper)
    for i in range(1, T):
        stat_copy(i).wait_send()
        mix_copy(i).wait_send()
        norm_copy(i).wait_send()
        for src in range(F):
            fin_copy(src, i).wait_send()


def solution(mesh):
    F, T = mesh.shape["fs"], mesh.shape["tp"]

    def step(tokens, norm_in, w_value, w_gate, conv_kernel, ln_gain, ln_shift, w_out, norm_mlp, w_up, w_down):
        S, D = tokens.shape
        R, C = w_value.shape
        H = w_up.shape[1]
        N = w_out.shape[1]
        rows = S // T
        chunks = 3 + 2 * PIECES
        bf16, f32 = jnp.bfloat16, jnp.float32
        dma = pltpu.SemaphoreType.DMA
        vmem = pl.BlockSpec(memory_space=pltpu.VMEM)
        anywhere = pl.BlockSpec(memory_space=pl.ANY)
        return pl.pallas_call(
            functools.partial(kernel, F, T),
            out_shape=jax.ShapeDtypeStruct((rows, D), bf16),
            in_specs=[vmem] * 6 + [anywhere] * 5,
            out_specs=vmem,
            scratch_shapes=[
                pltpu.VMEM((S, D), bf16),
                pltpu.VMEM((D, C), bf16),
                pltpu.VMEM((D, C), bf16),
                pltpu.VMEM((F, C, N), bf16),
                pltpu.VMEM((PIECES, D, H // PIECES), bf16),
                pltpu.VMEM((F, H, N), bf16),
                pltpu.VMEM((S + PAD, C), f32),
                pltpu.VMEM((S, C), f32),
                pltpu.VMEM((S, C), bf16),
                pltpu.VMEM((S, D), bf16),
                pltpu.VMEM((T, rows, D), bf16),
                pltpu.VMEM((rows, D), f32),
                pltpu.VMEM((S, D), bf16),
                pltpu.VMEM((S, H), bf16),
                pltpu.VMEM((F, S, N), bf16),
                pltpu.VMEM((F, T, rows, N), bf16),
                pltpu.VMEM((S, D), bf16),
                pltpu.VMEM((S, H - H // PIECES * (PIECES // 2)), bf16),
                pltpu.VMEM((F, S, N), bf16),
                pltpu.VMEM((F, T, rows, N), bf16),
                pltpu.VMEM((F, rows, N), bf16),
                pltpu.VMEM((F, rows, N), bf16),
                pltpu.VMEM((8, S), f32),
                pltpu.VMEM((T, 8, S), f32),
                pltpu.VMEM((rows, D), bf16),
                dma((4 + PIECES,)),
            ]
            + [dma((chunks, F))] * 8
            + [dma((T,))] * 6
            + [dma((F, T))] * 2
            + [dma((chunks,)), dma((2 + chunks,)), dma((T,)), dma((T,))]
            + [dma((F, T))] * 2
            + [dma((F,))] * 2,
            compiler_params=pltpu.CompilerParams(
                collective_id=0, has_side_effects=True, vmem_limit_bytes=62 * 1024 * 1024
            ),
        )(
            tokens, norm_in.reshape(1, D), conv_kernel, ln_gain.reshape(1, D), ln_shift.reshape(1, D),
            norm_mlp.reshape(1, D), w_value, w_gate, w_out, w_up, w_down,
        )

    in_specs = (
        P(("grp", "fs"), None), P(), P("fs", "tp"), P("fs", "tp"), P(), P(), P(),
        P("tp", "fs"), P(), P("fs", "tp"), P("tp", "fs"),
    )
    return jax.shard_map(
        step, mesh=mesh, in_specs=in_specs, out_specs=P(("grp", "fs", "tp"), None), check_vma=False
    )
```

profile of v0, /device:TPU:0, one launch (start us, length us, event | category | flops | bytes accessed | tf_op | source)
XLA Modules:
  0.0 206.1 jit_solution(6798131199136912077)
XLA Ops:
  0.0 1.3 reshape.12.norm_in
  1.3 1.3 reshape.13.ln_gain
  2.6 1.3 reshape.14.ln_shift
  3.9 1.3 reshape.15.norm_mlp
  5.1 199.1 %shard_map.109 = bf16[128,2048]{1,0:T(8,128)(2,1)} custom-call(bf16[512,2048]{1,0:T(8,128)(2,1)} %tok.1, bf16[1,2048]{1,0:T(2,128)(2,1)} %reshape.12.norm_in, f32[31,2048]{1,0:T(8,128)} %conv_k.1, bf16[1,2048]{1,0:T(2,128)(2,1)} %reshape.13.ln_gain, bf16[1,2048]{1,0:T(2,128)(2,1)} %reshape.14.ln_shift, bf16[1,2048]{1,0:T(2,128)(2,1)} %reshape.15.norm_mlp, ...), custom_call_target="tpu_custom_call" | custom-call | tf_op jit(solution)/shard_map/pallas_call | solution.py:611
  204.2 1.9 copy.13
where the time goes:
time: 206 us
  Pallas kernels  199 us (97%)
  local copies, waits for them, and re-layouts  7.03 us (3%)
    pallas_call x1, Pallas kernels, step(): pl.pallas_call(functools.partial(kernel, F, T), out_shape=jax.ShapeDtypeS...  199 us

commit v1 on v0

v1 whole, which is shorter than its diff:
```python
import functools

import jax
import jax.numpy as jnp
from jax import lax
from jax.experimental import pallas as pl
from jax.experimental.pallas import tpu as pltpu
from jax.sharding import PartitionSpec as P

MESH = pl.DeviceIdType.MESH
PIECES = 4
PAD = 32


def rms_rows(x, gain):
    return x * lax.rsqrt(jnp.mean(x * x, axis=-1, keepdims=True) + 1e-06) * gain


def groups_of(n):
    return 2 if n >= 512 else 1


def kernel(
    F, T,
    tok_h, norm_in, conv_h, ln_gain, ln_shift, norm_mlp, wv, wg, wo, wu, wd,
    out,
    tok, conv_k, normed, gv, gg, go, gu, gd, gated, conv, act, part, pr, rs, resid, nm, hidden, fin, fpr, rs2,
    sum_e, ret, st_own, st_recv, nm_own,
    local_sem, zsend_r, zsend_l, zrecv_r, zrecv_l, ysend_r, ysend_l, yrecv_r, yrecv_l,
    rest_send, rest_recv, st_send, st_rsem, md_send, md_recv, mx_send, mx_recv,
    agd_send, agd_recv, agx_send, agx_recv, give_sem, fd_send, fd_recv, fx_send, fx_recv, ret_send, ret_recv,
):
    g = lax.axis_index("grp")
    z = lax.axis_index("fs")
    t = lax.axis_index("tp")
    S, D = tok.shape
    R, C = wv.shape
    H = wu.shape[1]
    N = wo.shape[1]
    taps = conv_k.shape[0]
    rows = S // T
    half = T // 2
    R2, C2, H2 = R // 2, C // 2, H // 2
    HB = H // PIECES
    G = groups_of(N)
    subs = PIECES // G
    GC, HC = N // G, H2 // subs
    other = 1 - g
    n_chunks = 3 + 2 * PIECES
    first_down = 3 + PIECES
    core = lax.rem(t, 2)
    chip = lax.div(t, 2)
    partner = t + 1 - 2 * core

    at_left, at_right = z == 0, z == F - 1
    is_end = jnp.logical_or(at_left, at_right)
    not_end = jnp.logical_not(is_end)
    help_left, help_right = z == 1, z == F - 2

    def upper(c):
        return int(c >= 3)

    def has_rest(c):
        return c >= 1

    def when_right(c):
        return pl.when(z < F - 1 - upper(c))

    def when_left(c):
        return pl.when(z > 0 + upper(c))

    def for_ends(body):
        @pl.when(at_left)
        def _():
            body(z + 1)

        @pl.when(at_right)
        def _():
            body(z - 1)

    def for_helpers(body):
        @pl.when(help_left)
        def _():
            body(z - 1)

        @pl.when(help_right)
        def _():
            body(z + 1)

    def for_middle(body):
        @pl.when(not_end)
        def _():
            body()

    def mult(i, k):
        return pl.multiple_of(i, k)

    def own(c, h):
        if c < 3:
            ref, size = ((wv, R2), (wg, R2), (wo, C2))[c]
            return ref.at[pl.ds(mult(h * size, size), size), :]
        if c < first_down:
            return wu.at[pl.ds(mult(h * R2, R2), R2), pl.ds((c - 3) * HB, HB)]
        q, r = divmod(c - first_down, subs)
        return wd.at[pl.ds(mult(h * H2 + r * HC, HC), HC), pl.ds(q * GC, GC)]

    def slot(c, src, h):
        if c < 2:
            return (gv, gg)[c].at[pl.ds(mult(src * R + h * R2, R2), R2), :]
        if c == 2:
            return go.at[src, pl.ds(mult(h * C2, C2), C2), :]
        if c < first_down:
            return gu.at[c - 3, pl.ds(mult(src * R + h * R2, R2), R2), :]
        q, r = divmod(c - first_down, subs)
        return gd.at[src, q, pl.ds(mult(h * H2 + r * HC, HC), HC), :]

    def remote(src_ref, dst_ref, send, recv, device):
        return pltpu.make_async_remote_copy(
            src_ref=src_ref, dst_ref=dst_ref, send_sem=send, recv_sem=recv,
            device_id=device, device_id_type=MESH,
        )

    loads = [
        pltpu.make_async_copy(tok_h, tok, local_sem.at[0]),
        pltpu.make_async_copy(conv_h, conv_k, local_sem.at[1]),
    ]
    for copy in loads:
        copy.start()

    peers = [lax.rem(t + i, T) for i in range(T)]
    barrier = pltpu.get_barrier_semaphore()

    def greet(device):
        pl.semaphore_signal(barrier, inc=1, device_id=device, device_id_type=MESH)

    greet((other, z, t))
    for i in range(1, T):
        greet((g, z, peers[i]))

    @pl.when(z > 0)
    def _():
        greet((g, z - 1, t))

    @pl.when(z < F - 1)
    def _():
        greet((g, z + 1, t))

    ends = lax.div(z + F - 1, F) + lax.div(2 * F - 2 - z, F)
    with jax.named_scope("bar"):
        pl.semaphore_wait(barrier, T + ends)

    ys, yr = (ysend_r, ysend_l), (yrecv_r, yrecv_l)

    def own_right(c):
        return remote(own(c, g), slot(c, z, g), zsend_r.at[c, 0], zrecv_r.at[c, 1], (g, z + 1, t))

    def own_left(c):
        return remote(own(c, g), slot(c, z, g), zsend_l.at[c, 0], zrecv_l.at[c, 1], (g, z - 1, t))

    def right_hop(c, d, src):
        return remote(slot(c, src, g), slot(c, src, g), zsend_r.at[c, d], zrecv_r.at[c, min(d + 1, F - 1)], (g, z + 1, t))

    def left_hop(c, d, src):
        return remote(slot(c, src, g), slot(c, src, g), zsend_l.at[c, d], zrecv_l.at[c, min(d + 1, F - 1)], (g, z - 1, t))

    def arrival(c, d, src, left):
        sems = zrecv_l if left else zrecv_r
        return remote(slot(c, src, g), slot(c, src, g), zsend_r.at[c, d], sems.at[c, d], (other, z, t))

    def across(c, d, src, left):
        return remote(slot(c, src, g), slot(c, src, g), ys[left].at[c, d], yr[left].at[c, d], (other, z, t))

    def across_arrival(c, d, src, left):
        return remote(slot(c, src, other), slot(c, src, other), ys[left].at[c, d], yr[left].at[c, d], (other, z, t))

    def own_rest(c, helper):
        return remote(own(c, other), slot(c, z, other), rest_send.at[c], rest_recv.at[c], (g, helper, t))

    def own_send(c, act_on):
        @when_right(c)
        def _():
            act_on(own_right(c))

        @when_left(c)
        def _():
            act_on(own_left(c))

    def start(copy):
        copy.start()

    def sent(copy):
        copy.wait_send()

    def mid(c):
        for_middle(lambda: own_send(c, start))

    def end(c, first=True, second=True):
        @pl.when(is_end)
        def _():
            if first:
                own_send(c, start)
            if second and has_rest(c):
                for_ends(lambda helper: own_rest(c, helper).start())

    def both(d, body, c=0):
        @pl.when(jnp.logical_and(z - d >= 0, z < F - upper(c)))
        def _():
            body(z - d, 0)

        @pl.when(jnp.logical_and(z + d < F, z >= 0 + upper(c)))
        def _():
            body(z + d, 1)

    def when_across(c, d, left):
        if d > 1 or not has_rest(c):
            return lambda body: body()
        return pl.when(z != (F - 2 if left else 1))

    def forward(c, d, src, left, act_on):
        if d < F - 1:
            if left:
                @when_left(c)
                def _():
                    act_on(left_hop(c, d, src))
            else:
                @when_right(c)
                def _():
                    act_on(right_hop(c, d, src))

        @when_across(c, d, left)
        def _():
            act_on(across(c, d, src, left))

    def service(c, *ds):
        for d in ds:
            with jax.named_scope(f"S{c}_{d}"):
                def body(src, left):
                    arrival(c, d, src, left).wait_recv()
                    forward(c, d, src, left, start)

                both(d, body, c)

    far = range(2, F)

    def y_wait(c, *ds):
        for d in ds:
            with jax.named_scope(f"Y{c}_{d}"):
                def body(src, left):
                    @when_across(c, d, left)
                    def _():
                        across_arrival(c, d, src, left).wait_recv()

                    if d == 1 and has_rest(c):
                        @pl.when(z == (F - 2 if left else 1))
                        def _():
                            remote(slot(c, src, other), slot(c, src, other), rest_send.at[c], rest_recv.at[c], (g, src, t)).wait_recv()

                both(d, body, c)

    def drain(c):
        own_send(c, sent)
        if has_rest(c):
            for_ends(lambda helper: own_rest(c, helper).wait_send())
        for d in range(1, F):
            both(d, lambda src, left: forward(c, d, src, left, sent), c)

    mid(0)
    end(0)
    copies = [
        pltpu.make_async_copy(wv, gv.at[pl.ds(mult(z * R, R), R), :], local_sem.at[2]),
        pltpu.make_async_copy(wg, gg.at[pl.ds(mult(z * R, R), R), :], local_sem.at[3]),
        pltpu.make_async_copy(wo, go.at[z], local_sem.at[4]),
    ]
    for j in range(PIECES):
        copies.append(
            pltpu.make_async_copy(
                wu.at[:, pl.ds(j * HB, HB)], gu.at[j, pl.ds(mult(z * R, R), R), :], local_sem.at[5 + j]
            )
        )
    for q in range(G):
        copies.append(pltpu.make_async_copy(wd.at[:, pl.ds(q * GC, GC)], gd.at[z, q], local_sem.at[5 + PIECES + q]))
    end(1)
    end(2)
    for copy in copies:
        copy.start()
    for copy in loads:
        copy.wait()

    block = 64

    def norm_step(i, carry):
        at = pl.ds(mult(i * block, block), block)
        x = tok[at, :].astype(jnp.float32)
        normed[at, :] = rms_rows(x, norm_in[...].reshape(1, D).astype(jnp.float32)).astype(jnp.bfloat16)
        return carry

    with jax.named_scope("norm"):
        lax.fori_loop(0, S // block, norm_step, 0)
    for copy in copies:
        copy.wait()

    service(0, 1)
    mid(1)
    service(0, *far)
    end(3)
    service(1, 1)
    mid(2)
    mid(3)
    service(1, *far)
    end(4)
    service(2, 1)
    y_wait(0, *range(1, F))
    y_wait(1, *range(1, F))

    tile = min(256, C)
    gated[0:PAD, :] = jnp.zeros((PAD, C), jnp.float32)

    def gate_step(i, carry):
        at = pl.ds(mult(i * tile, tile), tile)
        v = jnp.dot(normed[...], gv[:, at], preferred_element_type=jnp.float32)
        a = jnp.dot(normed[...], gg[:, at], preferred_element_type=jnp.float32)
        gated[PAD:, at] = v * jax.nn.sigmoid(a)
        return carry

    with jax.named_scope("gate"):
        lax.fori_loop(0, C // tile, gate_step, 0)

    span = 128
    lead = PAD - (taps - 1)

    def conv_step(i, carry):
        base = mult(i * span, span)
        first = jnp.zeros((span, 128), jnp.float32)
        second = jnp.zeros((span, 128), jnp.float32)
        for j in range(C // 128):
            lanes = pl.ds(j * 128, 128)
            window = gated[pl.ds(base, span + PAD), lanes]
            weights = conv_k[:, pl.ds(mult(t * C + j * 128, 128), 128)]
            acc = jnp.zeros((span, 128), jnp.float32)
            for k in range(taps):
                acc = acc + weights[k : k + 1, :] * window[lead + k : lead + k + span, :]
            conv[pl.ds(base, span), lanes] = acc
            first = first + acc
            second = second + acc * acc
        lane = lax.broadcasted_iota(jnp.int32, (span, 128), 1)
        both_sums = jnp.where(
            lane == 0,
            jnp.sum(first, axis=1, keepdims=True),
            jnp.where(lane == 1, jnp.sum(second, axis=1, keepdims=True), 0.0),
        )
        st_own[:, pl.ds(base, span)] = jnp.transpose(both_sums)[0:8, :]
        return carry

    spans = S // span
    with jax.named_scope("conv_a"):
        lax.fori_loop(0, spans // 2, conv_step, 0)
    service(3, 1)
    mid(4)
    with jax.named_scope("conv_b"):
        lax.fori_loop(spans // 2, spans, conv_step, 0)

    def stat_copy(i):
        return remote(st_own, st_recv.at[i], st_send.at[i], st_rsem.at[i], (g, z, peers[i]))

    for i in range(1, T):
        stat_copy(i).start()
    service(2, *far)
    end(5)
    service(4, 1)
    mid(5)
    for i in range(1, T):
        stat_copy(i).wait_recv()

    gain = ln_gain[pl.ds(mult(t * C, C), C)].reshape(1, C).astype(jnp.float32)
    shift = ln_shift[pl.ds(mult(t * C, C), C)].reshape(1, C).astype(jnp.float32)

    def act_step(i, carry):
        base = mult(i * span, span)
        at = pl.ds(base, span)
        sums = st_own[:, at]
        for k in range(1, T):
            sums = sums + st_recv[k, :, at]
        mean = sums[0:1, :] / D
        var = sums[1:2, :] / D - mean * mean
        scale = lax.rsqrt(var + 1e-05)
        mean_c = jnp.transpose(jnp.broadcast_to(mean, (128, span)))[:, 0:1]
        scale_c = jnp.transpose(jnp.broadcast_to(scale, (128, span)))[:, 0:1]
        n = (conv[at, :] - mean_c) * scale_c * gain + shift
        act[at, :] = (n * jax.nn.sigmoid(n)).astype(jnp.bfloat16)
        return carry

    with jax.named_scope("act"):
        lax.fori_loop(0, S // span, act_step, 0)
    y_wait(2, *range(1, F))

    def put_rows(ref, cols, value):
        for r in range(T):
            ref[r % 2, (r // 2) * rows : (r // 2 + 1) * rows, cols] = value[r * rows : (r + 1) * rows, :]

    def row_block(j):
        return pl.ds(mult(j * rows, rows), rows)

    def mirror(i):
        return lax.rem(chip + i, half)

    def mirror_source(i):
        return lax.rem(chip - i + half, half)

    def mix_pair(i):
        cols = pl.ds(mult(i * N, N), N)
        return remote(part.at[1 - core, :, cols], pr.at[:, cols], md_send.at[i], md_recv.at[i], (g, z, partner))

    def mix_copy(i, m):
        cols = pl.ds(mult(i * N, N), N)
        return remote(
            part.at[core, row_block(mirror(m)), cols], rs.at[m, :, cols], mx_send.at[i, m], mx_recv.at[i, m],
            (g, z, 2 * mirror(m) + core),
        )

    def out_step(i, carry):
        value = jnp.dot(act[...], go[i], preferred_element_type=jnp.float32).astype(jnp.bfloat16)
        put_rows(part, pl.ds(mult(i * N, N), N), value)
        mix_pair(i).start()
        return carry

    with jax.named_scope("outp"):
        lax.fori_loop(0, F, out_step, 0)

    def pair_step(i, carry):
        mix_pair(i).wait_recv()
        cols = pl.ds(mult(i * N, N), N)
        for m in range(1, half):
            at = row_block(mirror(m))
            pair = part[core, at, cols].astype(jnp.float32) + pr[at, cols].astype(jnp.float32)
            part[core, at, cols] = pair.astype(jnp.bfloat16)
            mix_copy(i, m).start()
        return carry

    with jax.named_scope("mixpair"):
        lax.fori_loop(0, F, pair_step, 0)
    service(3, *far)
    end(6)
    service(5, 1)
    mid(6)
    service(4, *far)

    def mix_wait(i, carry):
        for m in range(1, half):
            mix_copy(i, m).wait_recv()
        return carry

    with jax.named_scope("mixw"):
        lax.fori_loop(0, F, mix_wait, 0)

    small = 32

    def resid_step(i, carry):
        at = pl.ds(mult(i * small, small), small)
        mine = pl.ds(mult(t * rows + i * small, small), small)
        held = pl.ds(mult(chip * rows + i * small, small), small)
        total = part[core, held, :].astype(jnp.float32) + pr[held, :].astype(jnp.float32)
        for m in range(1, half):
            total = total + rs[m, at, :].astype(jnp.float32)
        r = tok[mine, :].astype(jnp.float32) + total
        resid[at, :] = r
        nm_own[at, :] = rms_rows(r, norm_mlp[...].reshape(1, D).astype(jnp.float32)).astype(jnp.bfloat16)
        return carry

    with jax.named_scope("resid"):
        lax.fori_loop(0, rows // small, resid_step, 0)
    mine = row_block(t)

    def give_copy(helper):
        return remote(nm_own, nm.at[1, mine, :], give_sem.at[0], give_sem.at[1], (g, helper, t))

    for_ends(lambda helper: give_copy(helper).start())
    for c in range(first_down, n_chunks):
        end(c, second=False)
    for c in range(first_down, n_chunks):
        end(c, first=False)

    def gather_x(w, i):
        src = nm_own if w == 0 else nm.at[w, mine, :]
        return remote(src, nm.at[w, mine, :], agx_send.at[w, i], agx_recv.at[w, i], (g, z, 2 * mirror(i) + core))

    def gather_x_arrival(w, i):
        there = row_block(2 * mirror_source(i) + core)
        return remote(nm.at[w, there, :], nm.at[w, there, :], agx_send.at[w, i], agx_recv.at[w, i], (g, z, partner))

    def gather_d(w, i):
        if i == 0:
            src = nm_own if w == 0 else nm.at[w, mine, :]
            return remote(src, nm.at[w, mine, :], agd_send.at[w, 0], agd_recv.at[w, 0], (g, z, partner))
        there = row_block(2 * mirror_source(i) + core)
        return remote(nm.at[w, there, :], nm.at[w, there, :], agd_send.at[w, i], agd_recv.at[w, i], (g, z, partner))

    def gather_d_arrival(w, i):
        there = row_block(2 * mirror_source(i) + 1 - core)
        return remote(nm.at[w, there, :], nm.at[w, there, :], agd_send.at[w, i], agd_recv.at[w, i], (g, z, partner))

    def gather_start(w):
        for i in range(1, half):
            gather_x(w, i).start()
        gather_d(w, 0).start()

    def gather_pass(w):
        for i in range(1, half):
            gather_x_arrival(w, i).wait_recv()
            gather_d(w, i).start()

    def gather_wait(w):
        for i in range(half):
            gather_d_arrival(w, i).wait_recv()

    def gather_first():
        gather_start(0)
        nm[0, mine, :] = nm_own[...]

    for_middle(gather_first)
    service(6, 1)
    mid(7)
    service(5, *far)
    with jax.named_scope("gpass0"):
        for_middle(lambda: gather_pass(0))
    service(7, 1)
    mid(8)
    with jax.named_scope("gwait0"):
        for_middle(lambda: gather_wait(0))

    utile = min(256, HB)

    def up_block(w, j):
        def up_step(i, carry):
            at = pl.ds(mult(i * utile, utile), utile)
            a = jnp.dot(nm[w], gu[j, :, at], preferred_element_type=jnp.float32)
            a = jnp.maximum(a, 0.0)
            hidden[w, :, pl.ds(mult(j * HB + i * utile, utile), utile)] = (a * a).astype(jnp.bfloat16)
            return carry

        lax.fori_loop(0, HB // utile, up_step, 0)

    def up(j):
        y_wait(3 + j, *range(1, F))
        with jax.named_scope(f"up{j}"):
            for_middle(lambda: up_block(0, j))

    up(0)
    up(1)
    service(6, *far)
    up(2)
    service(8, 1)
    mid(9)
    up(3)

    def columns(q):
        return pl.ds(q * GC, GC)

    def fin_pair(w, q, src):
        return remote(
            fin.at[w, src, 1 - core, :, columns(q)], fpr.at[w, src, :, columns(q)],
            fd_send.at[w * F + src, q], fd_recv.at[w * F + src, q], (g, z, partner),
        )

    def fin_copy(w, q, src, m):
        return remote(
            fin.at[w, src, core, row_block(mirror(m)), columns(q)], rs2.at[w, src, m, :, columns(q)],
            fx_send.at[w * F + src, q * half + m], fx_recv.at[w * F + src, q * half + m],
            (g, z, 2 * mirror(m) + core),
        )

    def ret_copy(q, src, device):
        return remote(
            sum_e.at[src, :, columns(q)], ret.at[src, :, columns(q)], ret_send.at[src, q], ret_recv.at[src, q],
            (g, device, t),
        )

    def units(w, d, body):
        def run(*_):
            if d == 0:
                body(z)
                return

            def step(s, carry):
                body(z + (2 * s - 1) * d)
                return carry

            lax.fori_loop(1 - lax.div(z + F - d, F), 1 + lax.div(2 * F - 1 - z - d, F), step, 0)

        (for_helpers if w else for_middle)(run)

    def down(w, q, *ds):
        def body(src):
            value = jnp.dot(hidden[w], gd[src, q], preferred_element_type=jnp.float32).astype(jnp.bfloat16)
            put_rows(fin.at[w, src], columns(q), value)
            fin_pair(w, q, src).start()

        for d in ds:
            with jax.named_scope(f"down{w}{q}{d}"):
                units(w, d, body)

    def pair(w, q, *ds):
        def body(src):
            fin_pair(w, q, src).wait_recv()
            for m in range(1, half):
                at = row_block(mirror(m))
                total = fin[w, src, core, at, columns(q)].astype(jnp.float32) + fpr[w, src, at, columns(q)].astype(jnp.float32)
                fin[w, src, core, at, columns(q)] = total.astype(jnp.bfloat16)
                fin_copy(w, q, src, m).start()

        for d in ds:
            with jax.named_scope(f"pair{w}{q}{d}"):
                units(w, d, body)

    def finish(w, q, *ds):
        def body(src):
            for m in range(1, half):
                fin_copy(w, q, src, m).wait_recv()
            at = row_block(chip)
            total = fin[w, src, core, at, columns(q)].astype(jnp.float32) + fpr[w, src, at, columns(q)].astype(jnp.float32)
            for m in range(1, half):
                total = total + rs2[w, src, m, :, columns(q)].astype(jnp.float32)
            if w == 0:
                cols = pl.ds(mult(src * N + q * GC, GC), GC)
                out[:, cols] = (resid[:, cols] + total).astype(jnp.bfloat16)
            else:
                sum_e[src, :, columns(q)] = total.astype(jnp.bfloat16)
                for_helpers(lambda device: ret_copy(q, src, device).start())

        for d in ds:
            with jax.named_scope(f"fin{w}{q}{d}"):
                units(w, d, body)

    first_cols, last_cols = range(G - 1), G - 1

    for q in range(G):
        down(0, q, 0)

    def share(device):
        remote(nm_own, nm.at[1, mine, :], give_sem.at[0], give_sem.at[1], (g, device, t)).wait_recv()
        gather_start(1)

    with jax.named_scope("share"):
        for_helpers(share)
    service(7, *far)
    for q in range(G):
        pair(0, q, 0)
    service(9, 1)
    mid(10)
    service(8, *far)
    with jax.named_scope("gpass1"):
        for_helpers(lambda device: gather_pass(1))
    for c in range(first_down, first_down + subs * (G - 1)):
        y_wait(c, 1)
    for q in first_cols:
        down(0, q, 1)
    with jax.named_scope("gwait1"):
        for_helpers(lambda device: gather_wait(1))

    def up_end(lo, hi):
        def body(device):
            def step(j, carry):
                up_block(1, j)
                return carry

            lax.fori_loop(lo, hi, step, 0)

        with jax.named_scope("up_end"):
            for_helpers(body)

    up_end(0, PIECES // 2)
    service(10, 1)
    up_end(PIECES // 2, PIECES)
    service(9, *far)
    for q in first_cols:
        pair(0, q, 1)
    for q in range(G):
        down(1, q, 0)
    for q in first_cols:
        down(1, q, 1)
    for c in range(first_down, first_down + subs * (G - 1)):
        y_wait(c, *far)
    service(10, *far)
    for q in first_cols:
        down(0, q, *far)
        down(1, q, *far)
    for q in range(G):
        pair(1, q, 0)
    for q in first_cols:
        pair(1, q, 1)
        pair(0, q, *far)
        pair(1, q, *far)
    late = range(first_down + subs * (G - 1), n_chunks)
    for c in late:
        y_wait(c, 1)
    down(0, last_cols, 1)
    down(1, last_cols, 1)
    for c in range(first_down):
        drain(c)
    pair(0, last_cols, 1)
    pair(1, last_cols, 1)
    for q in range(G):
        finish(1, q, 0)
        finish(0, q, 0)
    for q in first_cols:
        finish(1, q, 1, *far)
        finish(0, q, 1, *far)
    for c in late:
        y_wait(c, *far)
    down(1, last_cols, *far)
    down(0, last_cols, *far)
    pair(1, last_cols, *far)
    pair(0, last_cols, *far)
    finish(1, last_cols, 1)
    finish(0, last_cols, 1)
    for c in range(first_down, n_chunks):
        drain(c)
    finish(1, last_cols, *far)
    finish(0, last_cols, *far)

    def take(helper):
        for q in range(G):
            def step(src, carry):
                ret_copy(q, src, helper).wait_recv()
                cols = pl.ds(mult(src * N + q * GC, GC), GC)
                out[:, cols] = (resid[:, cols] + ret[src, :, columns(q)].astype(jnp.float32)).astype(jnp.bfloat16)
                return carry

            lax.fori_loop(0, F, step, 0)

    with jax.named_scope("take"):
        for_ends(take)

    for_ends(lambda helper: give_copy(helper).wait_send())
    for i in range(1, T):
        stat_copy(i).wait_send()

    def drain_mix(i, carry):
        mix_pair(i).wait_send()
        for m in range(1, half):
            mix_copy(i, m).wait_send()
        return carry

    lax.fori_loop(0, F, drain_mix, 0)

    def drain_layer(w):
        for i in range(1, half):
            gather_x(w, i).wait_send()
        for i in range(half):
            gather_d(w, i).wait_send()

        def step(src, carry):
            for q in range(G):
                fin_pair(w, q, src).wait_send()
                for m in range(1, half):
                    fin_copy(w, q, src, m).wait_send()
                if w:
                    for_helpers(lambda device: ret_copy(q, src, device).wait_send())
            return carry

        lax.fori_loop(0, F, step, 0)

    for_middle(lambda: drain_layer(0))
    for_helpers(lambda device: drain_layer(1))


def solution(mesh):
    F, T = mesh.shape["fs"], mesh.shape["tp"]

    def step(tokens, norm_in, w_value, w_gate, conv_kernel, ln_gain, ln_shift, w_out, norm_mlp, w_up, w_down):
        S, D = tokens.shape
        R, C = w_value.shape
        H = w_up.shape[1]
        N = w_out.shape[1]
        rows, half, G = S // T, T // 2, groups_of(N)
        chunks = 3 + 2 * PIECES
        bf16, f32 = jnp.bfloat16, jnp.float32
        dma = pltpu.SemaphoreType.DMA
        vmem = pl.BlockSpec(memory_space=pltpu.VMEM)
        anywhere = pl.BlockSpec(memory_space=pl.ANY)
        return pl.pallas_call(
            functools.partial(kernel, F, T),
            out_shape=jax.ShapeDtypeStruct((rows, D), bf16),
            in_specs=[anywhere, vmem, anywhere, vmem, vmem, vmem] + [anywhere] * 5,
            out_specs=vmem,
            scratch_shapes=[
                pltpu.VMEM((S, D), bf16),
                pltpu.VMEM(conv_kernel.shape, f32),
                pltpu.VMEM((S, D), bf16),
                pltpu.VMEM((D, C), bf16),
                pltpu.VMEM((D, C), bf16),
                pltpu.VMEM((F, C, N), bf16),
                pltpu.VMEM((PIECES, D, H // PIECES), bf16),
                pltpu.VMEM((F, G, H, N // G), bf16),
                pltpu.VMEM((S + PAD, C), f32),
                pltpu.VMEM((S, C), f32),
                pltpu.VMEM((S, C), bf16),
                pltpu.VMEM((2, half * rows, D), bf16),
                pltpu.VMEM((half * rows, D), bf16),
                pltpu.VMEM((half, rows, D), bf16),
                pltpu.VMEM((rows, D), f32),
                pltpu.VMEM((2, S, D), bf16),
                pltpu.VMEM((2, S, H), bf16),
                pltpu.VMEM((2, F, 2, half * rows, N), bf16),
                pltpu.VMEM((2, F, half * rows, N), bf16),
                pltpu.VMEM((2, F, half, rows, N), bf16),
                pltpu.VMEM((F, rows, N), bf16),
                pltpu.VMEM((F, rows, N), bf16),
                pltpu.VMEM((8, S), f32),
                pltpu.VMEM((T, 8, S), f32),
                pltpu.VMEM((rows, D), bf16),
                dma((5 + PIECES + G,)),
            ]
            + [dma((chunks, F))] * 8
            + [dma((chunks,))] * 2
            + [dma((T,))] * 2
            + [dma((F,))] * 2
            + [dma((F, half))] * 2
            + [dma((2, half))] * 4
            + [dma((2,))]
            + [dma((2 * F, G))] * 2
            + [dma((2 * F, G * half))] * 2
            + [dma((F, G))] * 2,
            compiler_params=pltpu.CompilerParams(
                collective_id=0, has_side_effects=True, vmem_limit_bytes=62 * 1024 * 1024
            ),
        )(
            tokens, norm_in, conv_kernel, ln_gain, ln_shift, norm_mlp, w_value, w_gate, w_out, w_up, w_down,
        )

    in_specs = (
        P(("grp", "fs"), None), P(), P("fs", "tp"), P("fs", "tp"), P(), P(), P(),
        P("tp", "fs"), P(), P("fs", "tp"), P("tp", "fs"),
    )
    return jax.shard_map(
        step, mesh=mesh, in_specs=in_specs, out_specs=P(("grp", "fs", "tp"), None), check_vma=False
    )
```

time: 206 us -> 178 us (0.86)
  Pallas kernels: 199 us -> 176 us
  local copies, waits for them, and re-layouts: 7.03 us -> 1.88 us
    pallas_call x1, Pallas kernels: 199 us -> 176 us  [step(): pl.pallas_call(functools.partial(kernel, F, T), out_shape=jax.ShapeDtypeS...]
    reshape x4 -> x0, local copies, waits for them, and re-layouts: 5.14 us -> none  [the longest x1 1.29 us: step(): norm_in.reshape(1, D)]
where the time goes in v1:
time: 178 us
  Pallas kernels  176 us (99%)
  local copies, waits for them, and re-layouts  1.88 us (1%)
    pallas_call x1, Pallas kernels, step(): pl.pallas_call(functools.partial(kernel, F, T), out_shape=jax.ShapeDtypeS...  176 us

profile of v1, /device:TPU:0, one launch (start us, length us, event | category | flops | bytes accessed | tf_op | source)
XLA Modules:
  0.0 177.6 jit_solution(1850881630198166635)
XLA Ops:
  0.0 175.7 %shard_map.109 = bf16[128,2048]{1,0:T(8,128)(2,1)} custom-call(bf16[512,2048]{1,0:T(8,128)(2,1)} %tok_h.1, bf16[2048]{0:T(1024)(128)(2,1)} %norm_in.1, f32[31,2048]{1,0:T(8,128)} %conv_h.1, bf16[2048]{0:T(1024)(128)(2,1)} %ln_gain.1, bf16[2048]{0:T(1024)(128)(2,1)} %ln_shift.1, bf16[2048]{0:T(1024)(128)(2,1)} %norm_mlp.1, bf16[512,512]{1,0:T(8,128)(2,1)} %wv.1, ...), custom_call_target="tpu_custom_call" | custom-call | tf_op jit(solution)/shard_map/pallas_call | solution.py:780
  175.8 1.9 %copy.13 = bf16[128,2048]{1,0:T(8,128)(2,1)} copy(bf16[128,2048]{1,0:T(8,128)(2,1)} %shard_map.109) | data formatting | bytes 1048576

commit v2 on v1

--- a/solution.py
+++ b/solution.py
@@ -10,6 +10,7 @@
 MESH = pl.DeviceIdType.MESH
 PIECES = 4
 PAD = 32
+RING = 6
 
 
 def rms_rows(x, gain):
@@ -25,9 +26,8 @@
     tok_h, norm_in, conv_h, ln_gain, ln_shift, norm_mlp, wv, wg, wo, wu, wd,
     out,
     tok, conv_k, normed, gv, gg, go, gu, gd, gated, conv, act, part, pr, rs, resid, nm, hidden, fin, fpr, rs2,
-    sum_e, ret, st_own, st_recv, nm_own,
-    local_sem, zsend_r, zsend_l, zrecv_r, zrecv_l, ysend_r, ysend_l, yrecv_r, yrecv_l,
-    rest_send, rest_recv, st_send, st_rsem, md_send, md_recv, mx_send, mx_recv,
+    ret, st_own, st_recv, nm_own,
+    local_sem, own_sem, rest_sem, zsend, zrecv, ysend, yrecv, yrecv_all, st_send, st_rsem, md_send, md_recv, mx_send, mx_recv,
     agd_send, agd_recv, agx_send, agx_recv, give_sem, fd_send, fd_recv, fx_send, fx_recv, ret_send, ret_recv,
 ):
     g = lax.axis_index("grp")
@@ -40,7 +40,7 @@
     taps = conv_k.shape[0]
     rows = S // T
     half = T // 2
-    R2, C2, H2 = R // 2, C // 2, H // 2
+    R2, R4, C2, H2 = R // 2, R // 4, C // 2, H // 2
     HB = H // PIECES
     G = groups_of(N)
     subs = PIECES // G
@@ -48,6 +48,9 @@
     other = 1 - g
     n_chunks = 3 + 2 * PIECES
     first_down = 3 + PIECES
+    early = range(first_down, first_down + subs * (G - 1))
+    late = range(first_down + subs * (G - 1), n_chunks)
+    second = n_chunks
     core = lax.rem(t, 2)
     chip = lax.div(t, 2)
     partner = t + 1 - 2 * core
@@ -58,7 +61,7 @@
     help_left, help_right = z == 1, z == F - 2
 
     def upper(c):
-        return int(c >= 3)
+        return int(3 <= c < n_chunks)
 
     def has_rest(c):
         return c >= 1
@@ -72,11 +75,11 @@
     def for_ends(body):
         @pl.when(at_left)
         def _():
-            body(z + 1)
+            body(z + 1, 0)
 
         @pl.when(at_right)
         def _():
-            body(z - 1)
+            body(z - 1, 1)
 
     def for_helpers(body):
         @pl.when(help_left)
@@ -96,6 +99,8 @@
         return pl.multiple_of(i, k)
 
     def own(c, h):
+        if c in (0, second):
+            return wv.at[pl.ds(mult(h * R2 + (R4 if c else 0), R4), R4), :]
         if c < 3:
             ref, size = ((wv, R2), (wg, R2), (wo, C2))[c]
             return ref.at[pl.ds(mult(h * size, size), size), :]
@@ -105,8 +110,10 @@
         return wd.at[pl.ds(mult(h * H2 + r * HC, HC), HC), pl.ds(q * GC, GC)]
 
     def slot(c, src, h):
+        if c in (0, second):
+            return gv.at[pl.ds(mult(src * R + h * R2 + (R4 if c else 0), R4), R4), :]
         if c < 2:
-            return (gv, gg)[c].at[pl.ds(mult(src * R + h * R2, R2), R2), :]
+            return gg.at[pl.ds(mult(src * R + h * R2, R2), R2), :]
         if c == 2:
             return go.at[src, pl.ds(mult(h * C2, C2), C2), :]
         if c < first_down:
@@ -146,42 +153,71 @@
         greet((g, z + 1, t))
 
     ends = lax.div(z + F - 1, F) + lax.div(2 * F - 2 - z, F)
+    def greet_mirrors(there):
+        for m in range(1, half):
+            greet((g, there, 2 * lax.rem(chip + m, half) + core))
+
+    for_ends(lambda helper, left: greet_mirrors(helper))
+    for_helpers(greet_mirrors)
+    outer = lax.div(F + 1 - z, F) + lax.div(z + 2, F)
     with jax.named_scope("bar"):
-        pl.semaphore_wait(barrier, T + ends)
-
-    ys, yr = (ysend_r, ysend_l), (yrecv_r, yrecv_l)
+        pl.semaphore_wait(barrier, T + ends + (half - 1) * outer)
+
+    def index(d, left):
+        return d - 1 if left else F - 1 - d
+
+    order = (0, second, *range(1, n_chunks))
+
+    def ring(c):
+        return order.index(c) % RING
+
+    def before(c):
+        place = order.index(c) - RING
+        return order[place] if place >= 0 else None
+
+    def y_arrival(c, d, left):
+        if c in early or c in late:
+            return yrecv.at[c - first_down, index(d, left)]
+        return yrecv_all.at[order.index(c)]
 
     def own_right(c):
-        return remote(own(c, g), slot(c, z, g), zsend_r.at[c, 0], zrecv_r.at[c, 1], (g, z + 1, t))
+        return remote(own(c, g), slot(c, z, g), own_sem.at[ring(c), 0], zrecv.at[c, index(1, 0)], (g, z + 1, t))
 
     def own_left(c):
-        return remote(own(c, g), slot(c, z, g), zsend_l.at[c, 0], zrecv_l.at[c, 1], (g, z - 1, t))
-
-    def right_hop(c, d, src):
-        return remote(slot(c, src, g), slot(c, src, g), zsend_r.at[c, d], zrecv_r.at[c, min(d + 1, F - 1)], (g, z + 1, t))
-
-    def left_hop(c, d, src):
-        return remote(slot(c, src, g), slot(c, src, g), zsend_l.at[c, d], zrecv_l.at[c, min(d + 1, F - 1)], (g, z - 1, t))
+        return remote(own(c, g), slot(c, z, g), own_sem.at[ring(c), 1], zrecv.at[c, index(1, 1)], (g, z - 1, t))
+
+    def hop(c, d, src, left):
+        here = slot(c, src, g)
+        return remote(
+            here, here, zsend.at[ring(c), index(d, left)], zrecv.at[c, index(d + 1, left)], (g, z - 1 if left else z + 1, t)
+        )
 
     def arrival(c, d, src, left):
-        sems = zrecv_l if left else zrecv_r
-        return remote(slot(c, src, g), slot(c, src, g), zsend_r.at[c, d], sems.at[c, d], (other, z, t))
-
-    def across(c, d, src, left):
-        return remote(slot(c, src, g), slot(c, src, g), ys[left].at[c, d], yr[left].at[c, d], (other, z, t))
-
-    def across_arrival(c, d, src, left):
-        return remote(slot(c, src, other), slot(c, src, other), ys[left].at[c, d], yr[left].at[c, d], (other, z, t))
-
-    def own_rest(c, helper):
-        return remote(own(c, other), slot(c, z, other), rest_send.at[c], rest_recv.at[c], (g, helper, t))
-
-    def own_send(c, act_on):
-        @when_right(c)
+        here = slot(c, src, g)
+        return remote(here, here, zsend.at[ring(c), index(d, left)], zrecv.at[c, index(d, left)], (other, z, t))
+
+    def across(c, d, src, left, h=g):
+        here = slot(c, src, h)
+        return remote(here, here, ysend.at[ring(c), index(d, left)], y_arrival(c, d, left), (other, z, t))
+
+    def own_rest(c, helper, left):
+        return remote(own(c, other), slot(c, z, other), rest_sem.at[ring(c)], y_arrival(c, 1, left), (g, helper, t))
+
+    low = z < F // 2
+    high = jnp.logical_not(low)
+    upside = lax.div(z, F // 2)
+
+    def on_side(cond, left, side):
+        if side is None:
+            return cond
+        return jnp.logical_and(cond, high if bool(left) == (side == "near") else low)
+
+    def own_send(c, act_on, side=None):
+        @pl.when(on_side(z < F - 1 - upper(c), 1, side))
         def _():
             act_on(own_right(c))
 
-        @when_left(c)
+        @pl.when(on_side(z > 0 + upper(c), 0, side))
         def _():
             act_on(own_left(c))
 
@@ -191,23 +227,37 @@
     def sent(copy):
         copy.wait_send()
 
-    def mid(c):
-        for_middle(lambda: own_send(c, start))
-
-    def end(c, first=True, second=True):
+    def mid(c, side=None):
+        if before(c) is not None:
+            for_middle(lambda: own_send(before(c), sent, side))
+        for_middle(lambda: own_send(c, start, side))
+
+    def rest_send(c, act_on):
+        if has_rest(c):
+            for_ends(lambda helper, left: act_on(own_rest(c, helper, left)))
+
+    def end(c, first=True, rest=True):
         @pl.when(is_end)
         def _():
             if first:
+                if before(c) is not None:
+                    own_send(before(c), sent)
                 own_send(c, start)
-            if second and has_rest(c):
-                for_ends(lambda helper: own_rest(c, helper).start())
-
-    def both(d, body, c=0):
-        @pl.when(jnp.logical_and(z - d >= 0, z < F - upper(c)))
+            if rest:
+                if before(c) is not None:
+                    rest_send(before(c), sent)
+                rest_send(c, start)
+
+    def both(d, body, c=0, side=None, who=None):
+        def cond(base, left):
+            base = on_side(base, left, side)
+            return base if who is None else jnp.logical_and(base, is_end if who == "ends" else not_end)
+
+        @pl.when(cond(jnp.logical_and(z - d >= 0, z < F - upper(c)), 0))
         def _():
             body(z - d, 0)
 
-        @pl.when(jnp.logical_and(z + d < F, z >= 0 + upper(c)))
+        @pl.when(cond(jnp.logical_and(z + d < F, z >= 0 + upper(c)), 1))
         def _():
             body(z + d, 1)
 
@@ -218,54 +268,61 @@
 
     def forward(c, d, src, left, act_on):
         if d < F - 1:
-            if left:
-                @when_left(c)
-                def _():
-                    act_on(left_hop(c, d, src))
-            else:
-                @when_right(c)
-                def _():
-                    act_on(right_hop(c, d, src))
+            @(when_left if left else when_right)(c)
+            def _():
+                act_on(hop(c, d, src, left))
 
         @when_across(c, d, left)
         def _():
             act_on(across(c, d, src, left))
 
-    def service(c, *ds):
+    def service(c, *ds, side=None, who=None):
         for d in ds:
-            with jax.named_scope(f"S{c}_{d}"):
+            with jax.named_scope(f"S{c}_{d}{side or ''}"):
                 def body(src, left):
                     arrival(c, d, src, left).wait_recv()
                     forward(c, d, src, left, start)
 
-                both(d, body, c)
-
-    far = range(2, F)
-
-    def y_wait(c, *ds):
+                if before(c) is not None:
+                    both(d, lambda src, left: forward(before(c), d, src, left, sent), before(c), side, who)
+                both(d, body, c, side, who)
+
+    every, far = range(1, F), range(2, F)
+
+    def y_wait(c, *ds, side=None):
         for d in ds:
-            with jax.named_scope(f"Y{c}_{d}"):
+            with jax.named_scope(f"Y{c}_{d}{side or ''}"):
                 def body(src, left):
-                    @when_across(c, d, left)
-                    def _():
-                        across_arrival(c, d, src, left).wait_recv()
-
-                    if d == 1 and has_rest(c):
-                        @pl.when(z == (F - 2 if left else 1))
-                        def _():
-                            remote(slot(c, src, other), slot(c, src, other), rest_send.at[c], rest_recv.at[c], (g, src, t)).wait_recv()
-
-                both(d, body, c)
+                    across(c, d, src, left, other).wait_recv()
+
+                both(d, body, c, side)
+
+    def y_wait_all(c):
+        if c in (0, second):
+            got = gv.at[0 : (F - 1) * R4, :]
+        elif c < 3:
+            got = gg.at[0 : (F - 1) * R2, :] if c == 1 else go.at[0 : F - 1, 0:C2, :]
+        else:
+            got = gu.at[c - 3, 0 : (F - 1) * R2, :]
+
+        def body():
+            remote(got, got, yrecv_all.at[order.index(c)], yrecv_all.at[order.index(c)], (other, z, t)).wait_recv()
+
+        with jax.named_scope(f"Y{c}"):
+            for_middle(body) if upper(c) else body()
 
     def drain(c):
         own_send(c, sent)
-        if has_rest(c):
-            for_ends(lambda helper: own_rest(c, helper).wait_send())
+        rest_send(c, sent)
         for d in range(1, F):
             both(d, lambda src, left: forward(c, d, src, left, sent), c)
 
-    mid(0)
-    end(0)
+    for c in (0, second):
+        mid(c)
+        end(c, rest=False)
+    mid(1, "near")
+    end(1, rest=False)
+    end(2, rest=False)
     copies = [
         pltpu.make_async_copy(wv, gv.at[pl.ds(mult(z * R, R), R), :], local_sem.at[2]),
         pltpu.make_async_copy(wg, gg.at[pl.ds(mult(z * R, R), R), :], local_sem.at[3]),
@@ -279,8 +336,10 @@
         )
     for q in range(G):
         copies.append(pltpu.make_async_copy(wd.at[:, pl.ds(q * GC, GC)], gd.at[z, q], local_sem.at[5 + PIECES + q]))
-    end(1)
-    end(2)
+    end(second, first=False)
+    end(1, first=False)
+    end(2, first=False)
+    end(3)
     for copy in copies:
         copy.start()
     for copy in loads:
@@ -300,17 +359,25 @@
         copy.wait()
 
     service(0, 1)
-    mid(1)
+    service(second, 1)
+    mid(1, "far")
+    service(1, 1, side="near")
+    mid(2, "far")
+    service(1, 1, who="ends")
     service(0, *far)
-    end(3)
-    service(1, 1)
-    mid(2)
+    service(second, *far)
+    end(4)
+    service(1, 1, side="far", who="middle")
+    service(2, 1, side="near")
     mid(3)
+    mid(4)
     service(1, *far)
-    end(4)
-    service(2, 1)
-    y_wait(0, *range(1, F))
-    y_wait(1, *range(1, F))
+    mid(2, "near")
+    end(5)
+    service(2, 1, side="far")
+    y_wait_all(0)
+    y_wait_all(second)
+    y_wait_all(1)
 
     tile = min(256, C)
     gated[0:PAD, :] = jnp.zeros((PAD, C), jnp.float32)
@@ -352,22 +419,26 @@
         return carry
 
     spans = S // span
+    end(6)
+    service(2, *far, who="middle")
     with jax.named_scope("conv_a"):
         lax.fori_loop(0, spans // 2, conv_step, 0)
-    service(3, 1)
-    mid(4)
+    service(3, 1, side="near")
+    mid(5)
+    service(3, 1, side="far")
     with jax.named_scope("conv_b"):
         lax.fori_loop(spans // 2, spans, conv_step, 0)
 
     def stat_copy(i):
-        return remote(st_own, st_recv.at[i], st_send.at[i], st_rsem.at[i], (g, z, peers[i]))
+        return remote(st_own, st_recv.at[i], st_send.at[0], st_rsem.at[i], (g, z, peers[i]))
 
     for i in range(1, T):
         stat_copy(i).start()
-    service(2, *far)
-    end(5)
-    service(4, 1)
-    mid(5)
+    end(7, rest=False)
+    service(2, *far, who="ends")
+    service(4, 1, side="far")
+    service(4, 1, side="near")
+    mid(6)
     for i in range(1, T):
         stat_copy(i).wait_recv()
 
@@ -391,7 +462,7 @@
 
     with jax.named_scope("act"):
         lax.fori_loop(0, S // span, act_step, 0)
-    y_wait(2, *range(1, F))
+    y_wait_all(2)
 
     def put_rows(ref, cols, value):
         for r in range(T):
@@ -408,12 +479,12 @@
 
     def mix_pair(i):
         cols = pl.ds(mult(i * N, N), N)
-        return remote(part.at[1 - core, :, cols], pr.at[:, cols], md_send.at[i], md_recv.at[i], (g, z, partner))
+        return remote(part.at[1 - core, :, cols], pr.at[:, cols], md_send.at[0], md_recv.at[i], (g, z, partner))
 
     def mix_copy(i, m):
         cols = pl.ds(mult(i * N, N), N)
         return remote(
-            part.at[core, row_block(mirror(m)), cols], rs.at[m, :, cols], mx_send.at[i, m], mx_recv.at[i, m],
+            part.at[core, row_block(mirror(m)), cols], rs.at[m, :, cols], mx_send.at[0], mx_recv.at[i, m - 1],
             (g, z, 2 * mirror(m) + core),
         )
 
@@ -439,10 +510,9 @@
     with jax.named_scope("mixpair"):
         lax.fori_loop(0, F, pair_step, 0)
     service(3, *far)
-    end(6)
-    service(5, 1)
-    mid(6)
-    service(4, *far)
+    service(5, 1, side="far")
+    service(5, 1, side="near")
+    mid(7)
 
     def mix_wait(i, carry):
         for m in range(1, half):
@@ -473,30 +543,32 @@
     def give_copy(helper):
         return remote(nm_own, nm.at[1, mine, :], give_sem.at[0], give_sem.at[1], (g, helper, t))
 
-    for_ends(lambda helper: give_copy(helper).start())
-    for c in range(first_down, n_chunks):
-        end(c, second=False)
-    for c in range(first_down, n_chunks):
+    for_ends(lambda helper, left: give_copy(helper).start())
+    end(8, rest=False)
+    end(9, rest=False)
+    end(7, first=False)
+    end(10, rest=False)
+    for c in range(8, n_chunks):
         end(c, first=False)
 
     def gather_x(w, i):
         src = nm_own if w == 0 else nm.at[w, mine, :]
-        return remote(src, nm.at[w, mine, :], agx_send.at[w, i], agx_recv.at[w, i], (g, z, 2 * mirror(i) + core))
+        return remote(src, nm.at[w, mine, :], agx_send.at[w], agx_recv.at[w, i - 1], (g, z, 2 * mirror(i) + core))
 
     def gather_x_arrival(w, i):
         there = row_block(2 * mirror_source(i) + core)
-        return remote(nm.at[w, there, :], nm.at[w, there, :], agx_send.at[w, i], agx_recv.at[w, i], (g, z, partner))
+        return remote(nm.at[w, there, :], nm.at[w, there, :], agx_send.at[w], agx_recv.at[w, i - 1], (g, z, partner))
 
     def gather_d(w, i):
         if i == 0:
             src = nm_own if w == 0 else nm.at[w, mine, :]
-            return remote(src, nm.at[w, mine, :], agd_send.at[w, 0], agd_recv.at[w, 0], (g, z, partner))
+            return remote(src, nm.at[w, mine, :], agd_send.at[w], agd_recv.at[w, 0], (g, z, partner))
         there = row_block(2 * mirror_source(i) + core)
-        return remote(nm.at[w, there, :], nm.at[w, there, :], agd_send.at[w, i], agd_recv.at[w, i], (g, z, partner))
+        return remote(nm.at[w, there, :], nm.at[w, there, :], agd_send.at[w], agd_recv.at[w, i], (g, z, partner))
 
     def gather_d_arrival(w, i):
         there = row_block(2 * mirror_source(i) + 1 - core)
-        return remote(nm.at[w, there, :], nm.at[w, there, :], agd_send.at[w, i], agd_recv.at[w, i], (g, z, partner))
+        return remote(nm.at[w, there, :], nm.at[w, there, :], agd_send.at[w], agd_recv.at[w, i], (g, z, partner))
 
     def gather_start(w):
         for i in range(1, half):
@@ -517,13 +589,16 @@
         nm[0, mine, :] = nm_own[...]
 
     for_middle(gather_first)
-    service(6, 1)
-    mid(7)
+    service(4, *far)
+    service(6, 1, side="far")
+    service(6, 1, side="near")
+    mid(8)
     service(5, *far)
     with jax.named_scope("gpass0"):
         for_middle(lambda: gather_pass(0))
-    service(7, 1)
-    mid(8)
+    service(7, 1, side="far")
+    service(7, 1, side="near")
+    mid(9)
     with jax.named_scope("gwait0"):
         for_middle(lambda: gather_wait(0))
 
@@ -540,7 +615,7 @@
         lax.fori_loop(0, HB // utile, up_step, 0)
 
     def up(j):
-        y_wait(3 + j, *range(1, F))
+        y_wait_all(3 + j)
         with jax.named_scope(f"up{j}"):
             for_middle(lambda: up_block(0, j))
 
@@ -548,8 +623,14 @@
     up(1)
     service(6, *far)
     up(2)
-    service(8, 1)
-    mid(9)
+
+    def share(device):
+        remote(nm_own, nm.at[1, mine, :], give_sem.at[0], give_sem.at[1], (g, device, t)).wait_recv()
+        gather_start(1)
+
+    with jax.named_scope("share"):
+        for_helpers(share)
+    service(8, 1, side="far")
     up(3)
 
     def columns(q):
@@ -558,20 +639,20 @@
     def fin_pair(w, q, src):
         return remote(
             fin.at[w, src, 1 - core, :, columns(q)], fpr.at[w, src, :, columns(q)],
-            fd_send.at[w * F + src, q], fd_recv.at[w * F + src, q], (g, z, partner),
+            fd_send.at[w], fd_recv.at[w * F + src, q], (g, z, partner),
         )
 
-    def fin_copy(w, q, src, m):
+    def fin_copy(q, src, m):
         return remote(
-            fin.at[w, src, core, row_block(mirror(m)), columns(q)], rs2.at[w, src, m, :, columns(q)],
-            fx_send.at[w * F + src, q * half + m], fx_recv.at[w * F + src, q * half + m],
+            fin.at[0, src, core, row_block(mirror(m)), columns(q)], rs2.at[src, m, :, columns(q)],
+            fx_send.at[0], fx_recv.at[src, q * (half - 1) + m - 1],
             (g, z, 2 * mirror(m) + core),
         )
 
-    def ret_copy(q, src, device):
+    def ret_copy(q, src, m, device):
         return remote(
-            sum_e.at[src, :, columns(q)], ret.at[src, :, columns(q)], ret_send.at[src, q], ret_recv.at[src, q],
-            (g, device, t),
+            fin.at[1, src, core, row_block(mirror(m)), columns(q)], ret.at[m, src, :, columns(q)],
+            ret_send.at[0], ret_recv.at[src, q * half + m], (g, device, 2 * mirror(m) + core),
         )
 
     def units(w, d, body):
@@ -579,6 +660,9 @@
             if d == 0:
                 body(z)
                 return
+            if d in ("near", "far"):
+                body(z + (1 if d == "far" else -1) * (1 - 2 * upside))
+                return
 
             def step(s, carry):
                 body(z + (2 * s - 1) * d)
@@ -601,58 +685,53 @@
     def pair(w, q, *ds):
         def body(src):
             fin_pair(w, q, src).wait_recv()
-            for m in range(1, half):
+            for m in range(1 - w, half):
                 at = row_block(mirror(m))
                 total = fin[w, src, core, at, columns(q)].astype(jnp.float32) + fpr[w, src, at, columns(q)].astype(jnp.float32)
                 fin[w, src, core, at, columns(q)] = total.astype(jnp.bfloat16)
-                fin_copy(w, q, src, m).start()
+                if w:
+                    for_helpers(lambda device: ret_copy(q, src, m, device).start())
+                else:
+                    fin_copy(q, src, m).start()
 
         for d in ds:
             with jax.named_scope(f"pair{w}{q}{d}"):
                 units(w, d, body)
 
-    def finish(w, q, *ds):
+    def finish(q, *ds):
         def body(src):
             for m in range(1, half):
-                fin_copy(w, q, src, m).wait_recv()
+                fin_copy(q, src, m).wait_recv()
             at = row_block(chip)
-            total = fin[w, src, core, at, columns(q)].astype(jnp.float32) + fpr[w, src, at, columns(q)].astype(jnp.float32)
+            total = fin[0, src, core, at, columns(q)].astype(jnp.float32) + fpr[0, src, at, columns(q)].astype(jnp.float32)
             for m in range(1, half):
-                total = total + rs2[w, src, m, :, columns(q)].astype(jnp.float32)
-            if w == 0:
-                cols = pl.ds(mult(src * N + q * GC, GC), GC)
-                out[:, cols] = (resid[:, cols] + total).astype(jnp.bfloat16)
-            else:
-                sum_e[src, :, columns(q)] = total.astype(jnp.bfloat16)
-                for_helpers(lambda device: ret_copy(q, src, device).start())
+                total = total + rs2[src, m, :, columns(q)].astype(jnp.float32)
+            cols = pl.ds(mult(src * N + q * GC, GC), GC)
+            out[:, cols] = (resid[:, cols] + total).astype(jnp.bfloat16)
 
         for d in ds:
-            with jax.named_scope(f"fin{w}{q}{d}"):
-                units(w, d, body)
-
-    first_cols, last_cols = range(G - 1), G - 1
-
+            with jax.named_scope(f"fin{q}{d}"):
+                units(0, d, body)
+
+    first_cols, last = range(G - 1), G - 1
     for q in range(G):
         down(0, q, 0)
-
-    def share(device):
-        remote(nm_own, nm.at[1, mine, :], give_sem.at[0], give_sem.at[1], (g, device, t)).wait_recv()
-        gather_start(1)
-
-    with jax.named_scope("share"):
-        for_helpers(share)
-    service(7, *far)
     for q in range(G):
         pair(0, q, 0)
-    service(9, 1)
+    service(7, *far)
+    service(8, 1, side="near")
     mid(10)
-    service(8, *far)
+    service(9, 1, side="far")
+    for c in early:
+        y_wait(c, 1, side="far")
+    for q in first_cols:
+        down(0, q, "far")
     with jax.named_scope("gpass1"):
         for_helpers(lambda device: gather_pass(1))
-    for c in range(first_down, first_down + subs * (G - 1)):
-        y_wait(c, 1)
+    service(9, 1, side="near")
+    service(8, *far)
     for q in first_cols:
-        down(0, q, 1)
+        pair(0, q, "far")
     with jax.named_scope("gwait1"):
         for_helpers(lambda device: gather_wait(1))
 
@@ -667,62 +746,72 @@
         with jax.named_scope("up_end"):
             for_helpers(body)
 
-    up_end(0, PIECES // 2)
-    service(10, 1)
-    up_end(PIECES // 2, PIECES)
-    service(9, *far)
-    for q in first_cols:
-        pair(0, q, 1)
+    up_end(0, PIECES)
+    service(10, 1, side="far")
     for q in range(G):
         down(1, q, 0)
     for q in first_cols:
-        down(1, q, 1)
-    for c in range(first_down, first_down + subs * (G - 1)):
-        y_wait(c, *far)
-    service(10, *far)
-    for q in first_cols:
-        down(0, q, *far)
-        down(1, q, *far)
+        down(1, q, "far")
     for q in range(G):
         pair(1, q, 0)
     for q in first_cols:
-        pair(1, q, 1)
+        pair(1, q, "far")
+    service(10, 1, side="near")
+    for c in early:
+        y_wait(c, *far)
+    for q in first_cols:
+        down(1, q, *far)
+        down(0, q, *far)
+    service(9, *far)
+    for q in first_cols:
+        pair(1, q, *far)
         pair(0, q, *far)
-        pair(1, q, *far)
-    late = range(first_down + subs * (G - 1), n_chunks)
+    for c in early:
+        y_wait(c, 1, side="near")
+    for q in first_cols:
+        down(1, q, "near")
+        down(0, q, "near")
+    service(10, *far)
+    for q in first_cols:
+        pair(1, q, "near")
+        pair(0, q, "near")
     for c in late:
-        y_wait(c, 1)
-    down(0, last_cols, 1)
-    down(1, last_cols, 1)
-    for c in range(first_down):
-        drain(c)
-    pair(0, last_cols, 1)
-    pair(1, last_cols, 1)
+        y_wait(c, 1, side="far")
+    down(1, last, "far")
+    down(0, last, "far")
+    pair(1, last, "far")
+    pair(0, last, "far")
     for q in range(G):
-        finish(1, q, 0)
-        finish(0, q, 0)
+        finish(q, 0)
     for q in first_cols:
-        finish(1, q, 1, *far)
-        finish(0, q, 1, *far)
+        finish(q, "far", *far)
+        finish(q, "near")
+    for c in late:
+        y_wait(c, 1, side="near")
+    down(1, last, "near")
+    down(0, last, "near")
+    pair(1, last, "near")
+    pair(0, last, "near")
+    finish(last, "far")
     for c in late:
         y_wait(c, *far)
-    down(1, last_cols, *far)
-    down(0, last_cols, *far)
-    pair(1, last_cols, *far)
-    pair(0, last_cols, *far)
-    finish(1, last_cols, 1)
-    finish(0, last_cols, 1)
-    for c in range(first_down, n_chunks):
+    down(1, last, *far)
+    down(0, last, *far)
+    pair(1, last, *far)
+    pair(0, last, *far)
+    for c in order[-RING:]:
         drain(c)
-    finish(1, last_cols, *far)
-    finish(0, last_cols, *far)
-
-    def take(helper):
+    finish(last, "near", *far)
+
+    def take(helper, left):
         for q in range(G):
             def step(src, carry):
-                ret_copy(q, src, helper).wait_recv()
                 cols = pl.ds(mult(src * N + q * GC, GC), GC)
-                out[:, cols] = (resid[:, cols] + ret[src, :, columns(q)].astype(jnp.float32)).astype(jnp.bfloat16)
+                total = resid[:, cols]
+                for m in range(half):
+                    ret_copy(q, src, m, helper).wait_recv()
+                    total = total + ret[m, src, :, columns(q)].astype(jnp.float32)
+                out[:, cols] = total.astype(jnp.bfloat16)
                 return carry
 
             lax.fori_loop(0, F, step, 0)
@@ -730,37 +819,25 @@
     with jax.named_scope("take"):
         for_ends(take)
 
-    for_ends(lambda helper: give_copy(helper).wait_send())
-    for i in range(1, T):
-        stat_copy(i).wait_send()
-
-    def drain_mix(i, carry):
-        mix_pair(i).wait_send()
-        for m in range(1, half):
-            mix_copy(i, m).wait_send()
-        return carry
-
-    lax.fori_loop(0, F, drain_mix, 0)
-
-    def drain_layer(w):
-        for i in range(1, half):
-            gather_x(w, i).wait_send()
-        for i in range(half):
-            gather_d(w, i).wait_send()
-
-        def step(src, carry):
-            for q in range(G):
-                fin_pair(w, q, src).wait_send()
-                for m in range(1, half):
-                    fin_copy(w, q, src, m).wait_send()
-                if w:
-                    for_helpers(lambda device: ret_copy(q, src, device).wait_send())
-            return carry
-
-        lax.fori_loop(0, F, step, 0)
-
-    for_middle(lambda: drain_layer(0))
-    for_helpers(lambda device: drain_layer(1))
+    for_ends(lambda helper, left: give_copy(helper).wait_send())
+    def all_sent(ref, sem):
+        remote(ref, ref, sem, sem, (other, z, t)).wait_send()
+
+    all_sent(st_recv.at[1:T], st_send.at[0])
+    all_sent(pr, md_send.at[0])
+    all_sent(rs.at[1:half], mx_send.at[0])
+
+    def layer_sent(w):
+        all_sent(rs.at[1:half], agx_send.at[w])
+        all_sent(rs, agd_send.at[w])
+        all_sent(fpr.at[w], fd_send.at[w])
+        if w:
+            all_sent(ret, ret_send.at[0])
+        else:
+            all_sent(rs2.at[:, 1:half], fx_send.at[0])
+
+    for_middle(lambda: layer_sent(0))
+    for_helpers(lambda device: layer_sent(1))
 
 
 def solution(mesh):
@@ -772,7 +849,7 @@
         H = w_up.shape[1]
         N = w_out.shape[1]
         rows, half, G = S // T, T // 2, groups_of(N)
-        chunks = 3 + 2 * PIECES
+        chunks = 4 + 2 * PIECES
         bf16, f32 = jnp.bfloat16, jnp.float32
         dma = pltpu.SemaphoreType.DMA
         vmem = pl.BlockSpec(memory_space=pltpu.VMEM)
@@ -802,24 +879,18 @@
                 pltpu.VMEM((2, S, H), bf16),
                 pltpu.VMEM((2, F, 2, half * rows, N), bf16),
                 pltpu.VMEM((2, F, half * rows, N), bf16),
-                pltpu.VMEM((2, F, half, rows, N), bf16),
-                pltpu.VMEM((F, rows, N), bf16),
-                pltpu.VMEM((F, rows, N), bf16),
+                pltpu.VMEM((F, half, rows, N), bf16),
+                pltpu.VMEM((half, F, rows, N), bf16),
                 pltpu.VMEM((8, S), f32),
                 pltpu.VMEM((T, 8, S), f32),
                 pltpu.VMEM((rows, D), bf16),
                 dma((5 + PIECES + G,)),
             ]
-            + [dma((chunks, F))] * 8
-            + [dma((chunks,))] * 2
-            + [dma((T,))] * 2
-            + [dma((F,))] * 2
-            + [dma((F, half))] * 2
-            + [dma((2, half))] * 4
-            + [dma((2,))]
-            + [dma((2 * F, G))] * 2
-            + [dma((2 * F, G * half))] * 2
-            + [dma((F, G))] * 2,
+            + [dma((RING, 2)), dma((RING,))]
+            + [dma((RING, F - 1)), dma((chunks, F - 1)), dma((RING, F - 1)), dma((PIECES, F - 1)), dma((chunks - PIECES,))]
+            + [dma((1,)), dma((T,)), dma((1,)), dma((F,)), dma((1,)), dma((F, half - 1))]
+            + [dma((2,)), dma((2, half)), dma((2,)), dma((2, half - 1)), dma((2,))]
+            + [dma((2,)), dma((2 * F, G)), dma((1,)), dma((F, G * (half - 1))), dma((1,)), dma((F, G * half))],
             compiler_params=pltpu.CompilerParams(
                 collective_id=0, has_side_effects=True, vmem_limit_bytes=62 * 1024 * 1024
             ),

time: 178 us -> 153 us (0.86)
  Pallas kernels: 176 us -> 151 us
    pallas_call x1, Pallas kernels: 176 us -> 151 us  [step(): pl.pallas_call(functools.partial(kernel, F, T), out_shape=jax.ShapeDtypeS...]
where the time goes in v2:
time: 153 us
  Pallas kernels  151 us (99%)
  local copies, waits for them, and re-layouts  1.88 us (1%)
    pallas_call x1, Pallas kernels, step(): pl.pallas_call(functools.partial(kernel, F, T), out_shape=jax.ShapeDtypeS...  151 us

profile of v2, /device:TPU:0, one launch (start us, length us, event | category | flops | bytes accessed | tf_op | source)
XLA Modules:
  0.0 153.3 jit_solution(13803008458180119393)
XLA Ops:
  0.0 151.4 %shard_map.109 = bf16[128,2048]{1,0:T(8,128)(2,1)} custom-call(bf16[512,2048]{1,0:T(8,128)(2,1)} %tok_h.1, bf16[2048]{0:T(1024)(128)(2,1)} %norm_in.1, f32[31,2048]{1,0:T(8,128)} %conv_h.1, bf16[2048]{0:T(1024)(128)(2,1)} %ln_gain.1, bf16[2048]{0:T(1024)(128)(2,1)} %ln_shift.1, bf16[2048]{0:T(1024)(128)(2,1)} %norm_mlp.1, bf16[512,512]{1,0:T(8,128)(2,1)} %wv.1, ...), custom_call_target="tpu_custom_call" | custom-call | tf_op jit(solution)/shard_map/pallas_call | solution.py:857
  151.4 1.9 %copy.13 = bf16[128,2048]{1,0:T(8,128)(2,1)} copy(bf16[128,2048]{1,0:T(8,128)(2,1)} %shard_map.109) | data formatting | bytes 1048576

commit v3 on v2

--- a/solution.py
+++ b/solution.py
@@ -21,12 +21,17 @@
     return 2 if n >= 512 else 1
 
 
+def early_shape(f, s, n):
+    shape = (2, f, s, n // groups_of(n))
+    return shape if 4 * 2 * f * s * shape[3] <= 4 * 1024 * 1024 else (2, 1, 8, 128)
+
+
 def kernel(
     F, T,
     tok_h, norm_in, conv_h, ln_gain, ln_shift, norm_mlp, wv, wg, wo, wu, wd,
     out,
     tok, conv_k, normed, gv, gg, go, gu, gd, gated, conv, act, part, pr, rs, resid, nm, hidden, fin, fpr, rs2,
-    ret, st_own, st_recv, nm_own,
+    held, ret, st_own, st_recv, nm_own,
     local_sem, own_sem, rest_sem, zsend, zrecv, ysend, yrecv, yrecv_all, st_send, st_rsem, md_send, md_recv, mx_send, mx_recv,
     agd_send, agd_recv, agx_send, agx_recv, give_sem, fd_send, fd_recv, fx_send, fx_recv, ret_send, ret_recv,
 ):
@@ -178,6 +183,8 @@
     def y_arrival(c, d, left):
         if c in early or c in late:
             return yrecv.at[c - first_down, index(d, left)]
+        if c == 2:
+            return yrecv.at[PIECES, index(d, left)]
         return yrecv_all.at[order.index(c)]
 
     def own_right(c):
@@ -301,7 +308,7 @@
         if c in (0, second):
             got = gv.at[0 : (F - 1) * R4, :]
         elif c < 3:
-            got = gg.at[0 : (F - 1) * R2, :] if c == 1 else go.at[0 : F - 1, 0:C2, :]
+            got = gg.at[0 : (F - 1) * R2, :]
         else:
             got = gu.at[c - 3, 0 : (F - 1) * R2, :]
 
@@ -419,13 +426,14 @@
         return carry
 
     spans = S // span
-    end(6)
+    end(6, rest=False)
     service(2, *far, who="middle")
     with jax.named_scope("conv_a"):
         lax.fori_loop(0, spans // 2, conv_step, 0)
     service(3, 1, side="near")
     mid(5)
     service(3, 1, side="far")
+    service(2, 2, who="ends")
     with jax.named_scope("conv_b"):
         lax.fori_loop(spans // 2, spans, conv_step, 0)
 
@@ -434,8 +442,7 @@
 
     for i in range(1, T):
         stat_copy(i).start()
-    end(7, rest=False)
-    service(2, *far, who="ends")
+    service(2, *far[1:], who="ends")
     service(4, 1, side="far")
     service(4, 1, side="near")
     mid(6)
@@ -462,7 +469,6 @@
 
     with jax.named_scope("act"):
         lax.fori_loop(0, S // span, act_step, 0)
-    y_wait_all(2)
 
     def put_rows(ref, cols, value):
         for r in range(T):
@@ -488,27 +494,41 @@
             (g, z, 2 * mirror(m) + core),
         )
 
-    def out_step(i, carry):
+    def sources(d, body):
+        if d == 0:
+            body(z)
+            return
+
+        def step(s, carry):
+            body(z + (2 * s - 1) * d)
+            return carry
+
+        lax.fori_loop(1 - lax.div(z + F - d, F), 1 + lax.div(2 * F - 1 - z - d, F), step, 0)
+
+    def out_block(i):
         value = jnp.dot(act[...], go[i], preferred_element_type=jnp.float32).astype(jnp.bfloat16)
         put_rows(part, pl.ds(mult(i * N, N), N), value)
         mix_pair(i).start()
-        return carry
-
-    with jax.named_scope("outp"):
-        lax.fori_loop(0, F, out_step, 0)
-
-    def pair_step(i, carry):
+
+    def pair_block(i):
         mix_pair(i).wait_recv()
         cols = pl.ds(mult(i * N, N), N)
         for m in range(1, half):
             at = row_block(mirror(m))
-            pair = part[core, at, cols].astype(jnp.float32) + pr[at, cols].astype(jnp.float32)
-            part[core, at, cols] = pair.astype(jnp.bfloat16)
+            total = part[core, at, cols].astype(jnp.float32) + pr[at, cols].astype(jnp.float32)
+            part[core, at, cols] = total.astype(jnp.bfloat16)
             mix_copy(i, m).start()
-        return carry
-
-    with jax.named_scope("mixpair"):
-        lax.fori_loop(0, F, pair_step, 0)
+
+    for d in range(F):
+        if d:
+            y_wait(2, d)
+        with jax.named_scope(f"outp{d}"):
+            sources(d, out_block)
+        if d:
+            with jax.named_scope(f"mixpair{d - 1}"):
+                sources(d - 1, pair_block)
+    with jax.named_scope(f"mixpair{F - 1}"):
+        sources(F - 1, pair_block)
     service(3, *far)
     service(5, 1, side="far")
     service(5, 1, side="near")
@@ -527,8 +547,8 @@
     def resid_step(i, carry):
         at = pl.ds(mult(i * small, small), small)
         mine = pl.ds(mult(t * rows + i * small, small), small)
-        held = pl.ds(mult(chip * rows + i * small, small), small)
-        total = part[core, held, :].astype(jnp.float32) + pr[held, :].astype(jnp.float32)
+        kept = pl.ds(mult(chip * rows + i * small, small), small)
+        total = part[core, kept, :].astype(jnp.float32) + pr[kept, :].astype(jnp.float32)
         for m in range(1, half):
             total = total + rs[m, at, :].astype(jnp.float32)
         r = tok[mine, :].astype(jnp.float32) + total
@@ -544,6 +564,8 @@
         return remote(nm_own, nm.at[1, mine, :], give_sem.at[0], give_sem.at[1], (g, helper, t))
 
     for_ends(lambda helper, left: give_copy(helper).start())
+    end(7, rest=False)
+    end(6, first=False)
     end(8, rest=False)
     end(9, rest=False)
     end(7, first=False)
@@ -597,7 +619,6 @@
     with jax.named_scope("gpass0"):
         for_middle(lambda: gather_pass(0))
     service(7, 1, side="far")
-    service(7, 1, side="near")
     mid(9)
     with jax.named_scope("gwait0"):
         for_middle(lambda: gather_wait(0))
@@ -620,18 +641,22 @@
             for_middle(lambda: up_block(0, j))
 
     up(0)
+
+    def share(device):
+        remote(nm_own, nm.at[1, mine, :], give_sem.at[0], give_sem.at[1], (g, device, t)).wait_recv()
+        gather_start(1)
+
+    with jax.named_scope("share"):
+        for_helpers(share)
     up(1)
     service(6, *far)
     up(2)
-
-    def share(device):
-        remote(nm_own, nm.at[1, mine, :], give_sem.at[0], give_sem.at[1], (g, device, t)).wait_recv()
-        gather_start(1)
-
-    with jax.named_scope("share"):
-        for_helpers(share)
+    service(7, 1, side="near")
     service(8, 1, side="far")
     up(3)
+    with jax.named_scope("gpass1"):
+        for_helpers(lambda device: gather_pass(1))
+    service(9, 1, side="far")
 
     def columns(q):
         return pl.ds(q * GC, GC)
@@ -657,18 +682,10 @@
 
     def units(w, d, body):
         def run(*_):
-            if d == 0:
-                body(z)
-                return
             if d in ("near", "far"):
                 body(z + (1 if d == "far" else -1) * (1 - 2 * upside))
-                return
-
-            def step(s, carry):
-                body(z + (2 * s - 1) * d)
-                return carry
-
-            lax.fori_loop(1 - lax.div(z + F - d, F), 1 + lax.div(2 * F - 1 - z - d, F), step, 0)
+            else:
+                sources(d, body)
 
         (for_helpers if w else for_middle)(run)
 
@@ -680,6 +697,40 @@
 
         for d in ds:
             with jax.named_scope(f"down{w}{q}{d}"):
+                units(w, d, body)
+
+    tail = pl.ds(mult(other * H2 + (subs - 1) * HC, HC), HC)
+
+    starts_early = held.shape[1] == F
+
+    def down_part(w, *ds):
+        if not starts_early:
+            return
+
+        def body(src):
+            at = pl.ds(mult(g * H2, H2), H2)
+            total = jnp.dot(hidden[w, :, at], gd[src, G - 1, at, :], preferred_element_type=jnp.float32)
+            if subs > 1:
+                at = pl.ds(mult(other * H2, H2), (subs - 1) * HC)
+                total = total + jnp.dot(hidden[w, :, at], gd[src, G - 1, at, :], preferred_element_type=jnp.float32)
+            held[w, src] = total
+
+        for d in ds:
+            with jax.named_scope(f"dpart{w}{d}"):
+                units(w, d, body)
+
+    def down_rest(w, *ds):
+        if not starts_early:
+            down(w, G - 1, *ds)
+            return
+
+        def body(src):
+            total = held[w, src] + jnp.dot(hidden[w, :, tail], gd[src, G - 1, tail, :], preferred_element_type=jnp.float32)
+            put_rows(fin.at[w, src], columns(G - 1), total.astype(jnp.bfloat16))
+            fin_pair(w, G - 1, src).start()
+
+        for d in ds:
+            with jax.named_scope(f"drest{w}{d}"):
                 units(w, d, body)
 
     def pair(w, q, *ds):
@@ -716,22 +767,11 @@
     first_cols, last = range(G - 1), G - 1
     for q in range(G):
         down(0, q, 0)
+    service(7, *far)
     for q in range(G):
         pair(0, q, 0)
-    service(7, *far)
     service(8, 1, side="near")
     mid(10)
-    service(9, 1, side="far")
-    for c in early:
-        y_wait(c, 1, side="far")
-    for q in first_cols:
-        down(0, q, "far")
-    with jax.named_scope("gpass1"):
-        for_helpers(lambda device: gather_pass(1))
-    service(9, 1, side="near")
-    service(8, *far)
-    for q in first_cols:
-        pair(0, q, "far")
     with jax.named_scope("gwait1"):
         for_helpers(lambda device: gather_wait(1))
 
@@ -747,15 +787,21 @@
             for_helpers(body)
 
     up_end(0, PIECES)
-    service(10, 1, side="far")
+    service(8, *far)
     for q in range(G):
         down(1, q, 0)
+    service(9, 1, side="near")
+    for q in range(G):
+        pair(1, q, 0)
+    for c in early:
+        y_wait(c, 1, side="far")
     for q in first_cols:
         down(1, q, "far")
-    for q in range(G):
-        pair(1, q, 0)
+        down(0, q, "far")
+    service(10, 1, side="far")
     for q in first_cols:
         pair(1, q, "far")
+        pair(0, q, "far")
     service(10, 1, side="near")
     for c in early:
         y_wait(c, *far)
@@ -781,22 +827,28 @@
     down(0, last, "far")
     pair(1, last, "far")
     pair(0, last, "far")
+    for c in late[:-1]:
+        y_wait(c, 1, side="near")
+    down_part(1, "near")
+    down_part(0, "near")
     for q in range(G):
         finish(q, 0)
+    for c in late[:-1]:
+        y_wait(c, *far)
+    down_part(1, *far)
+    down_part(0, *far)
     for q in first_cols:
         finish(q, "far", *far)
         finish(q, "near")
-    for c in late:
-        y_wait(c, 1, side="near")
-    down(1, last, "near")
-    down(0, last, "near")
+    y_wait(late[-1], 1, side="near")
+    down_rest(1, "near")
+    down_rest(0, "near")
     pair(1, last, "near")
     pair(0, last, "near")
     finish(last, "far")
-    for c in late:
-        y_wait(c, *far)
-    down(1, last, *far)
-    down(0, last, *far)
+    y_wait(late[-1], *far)
+    down_rest(1, *far)
+    down_rest(0, *far)
     pair(1, last, *far)
     pair(0, last, *far)
     for c in order[-RING:]:
@@ -880,6 +932,7 @@
                 pltpu.VMEM((2, F, 2, half * rows, N), bf16),
                 pltpu.VMEM((2, F, half * rows, N), bf16),
                 pltpu.VMEM((F, half, rows, N), bf16),
+                pltpu.VMEM(early_shape(F, S, N), f32),
                 pltpu.VMEM((half, F, rows, N), bf16),
                 pltpu.VMEM((8, S), f32),
                 pltpu.VMEM((T, 8, S), f32),
@@ -887,12 +940,12 @@
                 dma((5 + PIECES + G,)),
             ]
             + [dma((RING, 2)), dma((RING,))]
-            + [dma((RING, F - 1)), dma((chunks, F - 1)), dma((RING, F - 1)), dma((PIECES, F - 1)), dma((chunks - PIECES,))]
+            + [dma((RING, F - 1)), dma((chunks, F - 1)), dma((RING, F - 1)), dma((PIECES + 1, F - 1)), dma((chunks - PIECES,))]
             + [dma((1,)), dma((T,)), dma((1,)), dma((F,)), dma((1,)), dma((F, half - 1))]
             + [dma((2,)), dma((2, half)), dma((2,)), dma((2, half - 1)), dma((2,))]
             + [dma((2,)), dma((2 * F, G)), dma((1,)), dma((F, G * (half - 1))), dma((1,)), dma((F, G * half))],
             compiler_params=pltpu.CompilerParams(
-                collective_id=0, has_side_effects=True, vmem_limit_bytes=62 * 1024 * 1024
+                collective_id=0, has_side_effects=True, vmem_limit_bytes=63 * 1024 * 1024
             ),
         )(
             tokens, norm_in, conv_kernel, ln_gain, ln_shift, norm_mlp, w_value, w_gate, w_out, w_up, w_down,

time: 153 us -> 153 us (level)
  no operation moved by 1% of the time
where the time goes in v3:
time: 153 us
  Pallas kernels  151 us (99%)
  local copies, waits for them, and re-layouts  1.88 us (1%)
    pallas_call x1, Pallas kernels, step(): pl.pallas_call(functools.partial(kernel, F, T), out_shape=jax.ShapeDtypeS...  151 us

profile of v3, /device:TPU:0, one launch (start us, length us, event | category | flops | bytes accessed | tf_op | source)
XLA Modules:
  0.0 152.5 jit_solution(17138368620988328791)
XLA Ops:
  0.0 150.7 %shard_map.109 = bf16[128,2048]{1,0:T(8,128)(2,1)} custom-call(bf16[512,2048]{1,0:T(8,128)(2,1)} %tok_h.1, bf16[2048]{0:T(1024)(128)(2,1)} %norm_in.1, f32[31,2048]{1,0:T(8,128)} %conv_h.1, bf16[2048]{0:T(1024)(128)(2,1)} %ln_gain.1, bf16[2048]{0:T(1024)(128)(2,1)} %ln_shift.1, bf16[2048]{0:T(1024)(128)(2,1)} %norm_mlp.1, bf16[512,512]{1,0:T(8,128)(2,1)} %wv.1, ...), custom_call_target="tpu_custom_call" | custom-call | tf_op jit(solution)/shard_map/pallas_call | solution.py:909
  150.7 1.9 %copy.13 = bf16[128,2048]{1,0:T(8,128)(2,1)} copy(bf16[128,2048]{1,0:T(8,128)(2,1)} %shard_map.109) | data formatting | bytes 1048576
